TPU v7x, 32 devices: a whole 2x2x4 slice. The times are simulated.
32 devices in a mesh: sp: 8 (over z, x), tp: 4 (over y, core).
Axes of the slice: x: 2, y: 2, z: 4, core: 2. Of those that a mesh axis runs over, the one named last changes fastest.
Arguments:
- latent: bfloat16 [6144, 2048], P(('sp', 'tp')), may hold values from -6 to 6
- context: bfloat16 [1024, 2048], P('sp'), may hold values from -6 to 6
- conditioning: float32 [2, 2048], replicated, may hold values from -6 to 6
- norm_gain: float32 [2048], replicated, may hold values from 0.1 to 1.9
- mod_shift: bfloat16 [2048, 2048], P('sp', 'tp'), may hold values from -0.1875 to 0.1875
- mod_scale: bfloat16 [2048, 2048], P('sp', 'tp'), may hold values from -0.1875 to 0.1875
- mod_gate: bfloat16 [2048, 2048], P('sp', 'tp'), may hold values from -0.1875 to 0.1875
- w_query: bfloat16 [2048, 2048], P(None, 'tp'), may hold values from -4 to 4
- w_key: bfloat16 [2048, 2048], P(None, 'tp'), may hold values from -0.125 to 0.125
- w_value: bfloat16 [2048, 2048], P(None, 'tp'), may hold values from -0.125 to 0.125
- w_out: bfloat16 [2048, 2048], P('tp'), may hold values from -0.125 to 0.125
- lambdas: float32 [16], P('tp'), may hold values from 0.3 to 0.8
- context_bias: float32 [16], P('tp'), may hold values from 0.8 to 2.2
- head_gain: float32 [128], replicated, may hold values from 0.1 to 1.9
Outputs:
- updated: bfloat16 [6144, 2048], P(('sp', 'tp'))
All inputs are finite; a program needn't handle non-finite values.
Results may differ from a plain program's by a relative error of at most 0.01.
The roundings to bfloat16 on the way count: a program that leaves them out, or rounds other values in their place, can miss the bound.
Values may be sent and summed in bfloat16 or wider, within the bound.
A program may use at most 128 MiB of HBM per device.

v0:
```python
import jax
import jax.numpy as jnp
from jax import lax
from jax.sharding import PartitionSpec as P

EPS = 1e-06
NEGATIVE = -1e30


def modulated(inputs, norm_scale, offset_vec, scale_vec):
    rows_float = inputs.astype(jnp.float32)
    normal = rows_float * lax.rsqrt(jnp.mean(rows_float * rows_float, axis=-1, keepdims=True) + EPS)
    return (normal * norm_scale * (1.0 + scale_vec) + offset_vec).astype(jnp.bfloat16)


def block_size(length):
    for candidate in range(min(length, 1024), 0, -1):
        if length % candidate == 0:
            return candidate
    return length


def absorb(running, portion, context_flags, queries, bias_heads):
    head_count = queries.shape[1]
    head_dim = queries.shape[3]
    row_count = portion.shape[0]
    head_cols = head_count * 2 * head_dim
    key_rows = portion[:, :head_cols].reshape(row_count, head_count, 2, head_dim)
    value_rows = portion[:, head_cols:].reshape(row_count, head_count, 2 * head_dim)
    shifts = bias_heads[:, None, None] * context_flags[None, None, :]
    updated = []
    for which_map in range(2):
        previous, weight, accumulated = running[3 * which_map : 3 * which_map + 3]
        scores = (
            jnp.einsum(
                "qhd,khd->hqk",
                queries[:, :, which_map],
                key_rows[:, :, which_map],
                preferred_element_type=jnp.float32,
            )
            * head_dim ** (-0.5)
            + shifts
        )
        peak_new = jnp.maximum(previous, jnp.max(scores, axis=2))
        faded = jnp.exp(previous - peak_new)
        raised = jnp.exp(scores - peak_new[:, :, None])
        weight = weight * faded + jnp.sum(raised, axis=2)
        accumulated = accumulated * faded.T[:, :, None] + jnp.einsum(
            "hqk,khd->qhd",
            raised.astype(jnp.bfloat16),
            value_rows,
            preferred_element_type=jnp.float32,
        )
        updated += [peak_new, weight, accumulated]
    return tuple(updated)


def absorb_rows(running, portion, context_flags, queries, bias_heads):
    row_count = portion.shape[0]
    block_len = block_size(row_count)
    if block_len == row_count:
        return absorb(running, portion, context_flags, queries, bias_heads)
    stacked = portion.reshape(row_count // block_len, block_len, portion.shape[1])
    flag_blocks = context_flags.reshape(row_count // block_len, block_len)

    def advance(state_now, operand):
        return (absorb(state_now, operand[0], operand[1], queries, bias_heads), None)

    running, unused = lax.scan(advance, running, (stacked, flag_blocks))
    return running


def per_device(
    latent,
    context,
    conditioning,
    norm_gain,
    mod_shift,
    mod_scale,
    mod_gate,
    w_query,
    w_key,
    w_value,
    w_out,
    lambdas,
    context_bias,
    head_gain,
):
    head_dim = head_gain.shape[0] // 2
    head_count = lambdas.shape[0]
    rows_sp = mod_shift.shape[0]
    cond_rows = lax.dynamic_slice_in_dim(conditioning, lax.axis_index("sp") * rows_sp, rows_sp, 1)
    activated = jax.nn.silu(cond_rows).astype(jnp.bfloat16)
    partials = jnp.stack(
        [
            jnp.dot(activated, matrix, preferred_element_type=jnp.float32)
            for matrix in (mod_shift, mod_scale, mod_gate)
        ],
        axis=1,
    )
    summed = lax.psum(partials, "sp")
    modulation = lax.all_gather(summed, "tp", axis=2, tiled=True)
    own_rows = modulated(latent, norm_gain, modulation[0, 0], modulation[0, 1])
    context_rows = modulated(context, norm_gain, modulation[1, 0], modulation[1, 1])
    key_value = jnp.concatenate([w_key, w_value], axis=1)
    projector = jnp.concatenate([w_query, key_value], axis=1)
    projected = jnp.dot(
        lax.all_gather(own_rows, "tp", axis=0, tiled=True),
        projector,
        preferred_element_type=jnp.float32,
    ).astype(jnp.bfloat16)
    head_cols = w_query.shape[1]
    token_count = projected.shape[0]
    queries = projected[:, :head_cols].reshape(token_count, head_count, 2, head_dim)
    latent_kv = projected[:, head_cols:]
    context_kv = jnp.dot(context_rows, key_value, preferred_element_type=jnp.float32).astype(
        jnp.bfloat16
    )
    first_map = (
        jnp.full((head_count, token_count), NEGATIVE, jnp.float32),
        jnp.zeros((head_count, token_count), jnp.float32),
        jnp.zeros((token_count, head_count, 2 * head_dim), jnp.float32),
    )
    initial = first_map + first_map
    every_context = lax.all_gather(context_kv, "sp", axis=0, tiled=True)
    running = absorb_rows(
        initial,
        every_context,
        jnp.ones((every_context.shape[0],), jnp.float32),
        queries,
        context_bias,
    )
    portion = lax.all_gather(latent_kv, "sp", axis=0, tiled=True)
    running = absorb_rows(
        running, portion, jnp.zeros((portion.shape[0],), jnp.float32), queries, context_bias
    )
    peak_one, total_one, accum_one, peak_two, total_two, accum_two = running
    mixed = accum_one / total_one.T[:, :, None] - lambdas[None, :, None] * (
        accum_two / total_two.T[:, :, None]
    )
    normed = mixed * lax.rsqrt(jnp.mean(mixed * mixed, axis=-1, keepdims=True) + EPS) * head_gain
    flattened = normed.reshape(token_count, head_cols).astype(jnp.bfloat16)
    attended = lax.psum_scatter(
        jnp.dot(flattened, w_out, preferred_element_type=jnp.float32).astype(jnp.bfloat16),
        "tp",
        scatter_dimension=0,
        tiled=True,
    )
    return (latent.astype(jnp.float32) + modulation[0, 2] * attended.astype(jnp.float32)).astype(
        jnp.bfloat16
    )


def solution(mesh):
    return jax.shard_map(
        per_device,
        mesh=mesh,
        in_specs=(
            P(("sp", "tp"), None),
            P("sp", None),
            P(),
            P(),
            P("sp", "tp"),
            P("sp", "tp"),
            P("sp", "tp"),
            P(None, "tp"),
            P(None, "tp"),
            P(None, "tp"),
            P("tp", None),
            P("tp"),
            P("tp"),
            P(),
        ),
        out_specs=P(("sp", "tp"), None),
        check_vma=False,
    )
```

profile of v0, /device:TPU:0, one launch (start us, length us, event | category | flops | bytes accessed | tf_op | source)
XLA Modules:
  0.0 557.7 jit_solution(13907041467783386179)
XLA Ops:
  10.0 38.8 %psum.7 = f32[2,3,512]{2,0,1:T(2,128)S(1)} all-reduce(f32[2,3,512]{2,0,1:T(2,128)S(1)} %pad_maximum_fusion), channel_id=1, replica_groups=mesh['sp'=8,'tp'=4] {'sp'}, use_global_device_ids=true, to_apply=%region_0.1 | all-reduce | flops 3072 | bytes 24576 | tf_op jit(solution)/shard_map/psum | solution.py:101
  48.9 5.2 all_gather.12
  59.8 4.0 fusion.57
  63.9 20.6 %all-gather.4.cloned.1.call-done = bf16[768,2048]{1,0:T(8,128)(2,1)} async-done(((bf16[192,2048]{1,0:T(8,128)(2,1)}), bf16[768,2048]{1,0:T(8,128)(2,1)}) %all-gather.4.cloned.1.call-update) | async-done | bytes 3145744 | tf_op jit(solution)/shard_map/all_gather | solution.py:108
  84.5 8.8 %fusion.44 = bf16[768,1536]{1,0:T(8,128)(2,1)S(1)} fusion(bf16[768,2048]{1,0:T(8,128)(2,1)} %all-gather.4.cloned.1.call-done, bf16[2048,512]{1,0:T(8,128)(2,1)} %param.25, bf16[2048,512]{1,0:T(8,128)(2,1)} %param.24, bf16[2048,512]{1,0:T(8,128)(2,1)} %param.23), kind=kOutput, calls=%fused_computation.56 | convolution fusion | flops 4851892224 | bytes 11796480 | tf_op jit(solution)/shard_map/dot_general | solution.py:107
  96.4 39.3 %all-gather.6.cloned.1.call-done = bf16[1024,1024]{1,0:T(8,128)(2,1)} async-done(((bf16[128,1024]{1,0:T(8,128)(2,1)}), bf16[1024,1024]{1,0:T(8,128)(2,1)}) %all-gather.6.cloned.1.call-update) | async-done | bytes 2097168 | tf_op jit(solution)/shard_map/all_gather | solution.py:125
  135.7 2.7 fusion.85
  146.5 3.1 fusion.67
  149.7 6.2 %fusion.25 = (f32[4,768]{1,0:T(4,128)S(1)}, f32[4,768]{1,0:T(4,128)S(1)}, f32[4,768,1024]{2,1,0:T(8,128)}) fusion(f32[4]{0:T(128)S(1)} %copy-done.9, f32[4,768,1024]{2,1,0:T(8,128)S(1)} %fusion.67, bf16[1024,4,2,64]{0,3,2,1:T(8,128)(2,1)S(1)} %bitcast.155, bf16[768,4,2,64]{0,3,2,1:T(8,128)(2,1)S(1)} %bitcast.153), kind=kOutput, calls=%fused_computation.39 | convolution fusion | flops 421521408 | bytes 26108416 | tf_op jit(solution)/shard_map/qhd,khd->hqk/dot_general | solution.py:35
  155.8 8.2 %fusion.29 = (f32[4,768]{1,0:T(4,128)S(1)}, f32[4,768]{1,0:T(4,128)S(1)}) fusion(f32[4,768,1024]{2,1,0:T(8,128)} %get-tuple-element.134, f32[4,768]{1,0:T(4,128)S(1)} %broadcast_maximum_fusion, f32[4]{0:T(128)S(1)} %copy-done.9, f32[4,768]{1,0:T(4,128)S(1)} %broadcast_maximum_fusion.1, f32[4,768,1024]{2,1,0:T(8,128)S(1)} %fusion.67), kind=kLoop, calls=%fused_computation.43 | loop fusion | flops 25159680 | bytes 25214992 | tf_op jit(solution)/shard_map/reduce_sum | solution.py:47
  164.0 8.6 %bitcast_add_fusion.2 = f32[768,4,128]{0,2,1:T(8,128)} fusion(bf16[1024,4,128]{0,2,1:T(8,128)(2,1)S(1)} %bitcast.156, f32[4,768,1024]{2,1,0:T(8,128)} %get-tuple-element.134, f32[4,768]{1,0:T(4,128)S(1)} %broadcast_maximum_fusion, f32[4]{0:T(128)S(1)} %copy-done.9, f32[768,4]{0,1:T(4,128)S(1)} %get-tuple-element.136), kind=kOutput, calls=%fused_computation.67 | convolution fusion | flops 818282496 | bytes 15228944 | tf_op jit(solution)/shard_map/hqk,khd->qhd/dot_general | solution.py:48
  172.7 4.1 bitcast_add_fusion.3
  176.8 135.7 %all-gather.8.cloned.1.call-done = bf16[6144,1024]{1,0:T(8,128)(2,1)} async-done(((bf16[768,1024]{1,0:T(8,128)(2,1)}), bf16[6144,1024]{1,0:T(8,128)(2,1)}) %all-gather.8.cloned.1.call-update) | async-done | bytes 12582928 | tf_op jit(solution)/shard_map/all_gather | solution.py:133
  312.6 193.9 %while.20 = (s32[]{:T(128)}, f32[4,768]{1,0:T(4,128)S(1)}, f32[4,768]{1,0:T(4,128)S(1)}, f32[768,4,128]{0,2,1:T(8,128)}, f32[4,768]{1,0:T(4,128)S(1)}, /*index=5...) while((s32[]{:T(128)}, f32[4,768]{1,0:T(4,128)S(1)}, ...), condition=%wide.region_12.13_spmd, body=%wide.region_7.12_spmd.sunk | while | flops 2486716416 | bytes 128058136 | solution.py:69
  312.6 3.1 constant_dynamic-slice_fusion.2
  315.7 3.9 copy.54
  319.6 2.7 fusion.114
  322.3 2.8 fusion.115
  325.1 5.5 bitcast_reduce_fusion.3
  330.7 5.8 %bitcast_add_fusion.7 = f32[768,4,128]{0,2,1:T(8,128)} fusion(f32[768,4,128]{0,2,1:T(8,128)} %get-tuple-element.241, bf16[1024,4,128]{0,2,1:T(8,128)(2,1)} %bitcast.148, f32[4,1024,768]{2,1,0:T(8,128)S(1)} %get-tuple-element.214, f32[4,768]{1,0:T(4,128)S(1)} %get-tuple-element.250, f32[4]{0:T(128)S(1)} %broadcast_multiply_fusion.2, ...), kind=kOutput, calls=%fused_computation.14.clone.1 | convolution fusion | flops 818675712 | bytes 16801808 | tf_op jit(solution)/shard_map/while/body/eval_jaxpr/hqk,khd->qhd/dot_general | solution.py:48
  336.5 3.2 bitcast_add_fusion.6
  339.7 5.1 fusion.118
  344.9 3.1 constant_dynamic-slice_fusion.2
  348.0 3.9 copy.54
  351.9 2.7 fusion.114
  354.6 2.8 fusion.115
  357.5 5.5 bitcast_reduce_fusion.3
  363.0 5.8 %bitcast_add_fusion.7 = f32[768,4,128]{0,2,1:T(8,128)} fusion(f32[768,4,128]{0,2,1:T(8,128)} %get-tuple-element.241, bf16[1024,4,128]{0,2,1:T(8,128)(2,1)} %bitcast.148, f32[4,1024,768]{2,1,0:T(8,128)S(1)} %get-tuple-element.214, f32[4,768]{1,0:T(4,128)S(1)} %get-tuple-element.250, f32[4]{0:T(128)S(1)} %broadcast_multiply_fusion.2, ...), kind=kOutput, calls=%fused_computation.14.clone.1 | convolution fusion | flops 818675712 | bytes 16801808 | tf_op jit(solution)/shard_map/while/body/eval_jaxpr/hqk,khd->qhd/dot_general | solution.py:48
  368.8 3.2 bitcast_add_fusion.6
  372.0 5.1 fusion.118
  377.2 3.1 constant_dynamic-slice_fusion.2
  380.3 3.9 copy.54
  384.2 2.7 fusion.114
  386.9 2.8 fusion.115
  389.8 5.5 bitcast_reduce_fusion.3
  395.3 5.8 %bitcast_add_fusion.7 = f32[768,4,128]{0,2,1:T(8,128)} fusion(f32[768,4,128]{0,2,1:T(8,128)} %get-tuple-element.241, bf16[1024,4,128]{0,2,1:T(8,128)(2,1)} %bitcast.148, f32[4,1024,768]{2,1,0:T(8,128)S(1)} %get-tuple-element.214, f32[4,768]{1,0:T(4,128)S(1)} %get-tuple-element.250, f32[4]{0:T(128)S(1)} %broadcast_multiply_fusion.2, ...), kind=kOutput, calls=%fused_computation.14.clone.1 | convolution fusion | flops 818675712 | bytes 16801808 | tf_op jit(solution)/shard_map/while/body/eval_jaxpr/hqk,khd->qhd/dot_general | solution.py:48
  401.1 3.2 bitcast_add_fusion.6
  404.3 5.1 fusion.118
  409.5 3.1 constant_dynamic-slice_fusion.2
  412.6 3.9 copy.54
  416.6 2.7 fusion.114
  419.3 2.8 fusion.115
  422.1 5.5 bitcast_reduce_fusion.3
  427.6 5.8 %bitcast_add_fusion.7 = f32[768,4,128]{0,2,1:T(8,128)} fusion(f32[768,4,128]{0,2,1:T(8,128)} %get-tuple-element.241, bf16[1024,4,128]{0,2,1:T(8,128)(2,1)} %bitcast.148, f32[4,1024,768]{2,1,0:T(8,128)S(1)} %get-tuple-element.214, f32[4,768]{1,0:T(4,128)S(1)} %get-tuple-element.250, f32[4]{0:T(128)S(1)} %broadcast_multiply_fusion.2, ...), kind=kOutput, calls=%fused_computation.14.clone.1 | convolution fusion | flops 818675712 | bytes 16801808 | tf_op jit(solution)/shard_map/while/body/eval_jaxpr/hqk,khd->qhd/dot_general | solution.py:48
  433.4 3.2 bitcast_add_fusion.6
  436.6 5.1 fusion.118
  441.9 3.1 constant_dynamic-slice_fusion.2
  445.0 3.9 copy.54
  448.9 2.7 fusion.114
  451.6 2.8 fusion.115
  454.4 5.5 bitcast_reduce_fusion.3
  459.9 5.8 %bitcast_add_fusion.7 = f32[768,4,128]{0,2,1:T(8,128)} fusion(f32[768,4,128]{0,2,1:T(8,128)} %get-tuple-element.241, bf16[1024,4,128]{0,2,1:T(8,128)(2,1)} %bitcast.148, f32[4,1024,768]{2,1,0:T(8,128)S(1)} %get-tuple-element.214, f32[4,768]{1,0:T(4,128)S(1)} %get-tuple-element.250, f32[4]{0:T(128)S(1)} %broadcast_multiply_fusion.2, ...), kind=kOutput, calls=%fused_computation.14.clone.1 | convolution fusion | flops 818675712 | bytes 16801808 | tf_op jit(solution)/shard_map/while/body/eval_jaxpr/hqk,khd->qhd/dot_general | solution.py:48
  465.7 3.2 bitcast_add_fusion.6
  469.0 5.1 fusion.118
  474.2 3.1 constant_dynamic-slice_fusion.2
  477.3 3.9 copy.54
  481.2 2.7 fusion.114
  483.9 2.8 fusion.115
  486.7 5.5 bitcast_reduce_fusion.3
  492.3 5.8 %bitcast_add_fusion.7 = f32[768,4,128]{0,2,1:T(8,128)} fusion(f32[768,4,128]{0,2,1:T(8,128)} %get-tuple-element.241, bf16[1024,4,128]{0,2,1:T(8,128)(2,1)} %bitcast.148, f32[4,1024,768]{2,1,0:T(8,128)S(1)} %get-tuple-element.214, f32[4,768]{1,0:T(4,128)S(1)} %get-tuple-element.250, f32[4]{0:T(128)S(1)} %broadcast_multiply_fusion.2, ...), kind=kOutput, calls=%fused_computation.14.clone.1 | convolution fusion | flops 818675712 | bytes 16801808 | tf_op jit(solution)/shard_map/while/body/eval_jaxpr/hqk,khd->qhd/dot_general | solution.py:48
  498.1 3.2 bitcast_add_fusion.6
  501.3 5.1 fusion.118
  509.1 3.5 convolution_convert_fusion
  512.7 36.2 %reduce-scatter.2.cloned.1.call-done = bf16[192,2048]{1,0:T(8,128)(2,1)} async-done(((bf16[768,2048]{1,0:T(8,128)(2,1)}), bf16[192,2048]{1,0:T(8,128)(2,1)}) %reduce-scatter.2.cloned.1.call-update) | async-done | bytes 786448 | tf_op jit(solution)/shard_map/reduce_scatter | solution.py:143
  (121 shorter events, 26.0 us)
Async XLA Ops:
  6.5 502.6 %copy-start = (bf16[512,2048]{1,0:T(8,128)(2,1)S(1)}, bf16[512,2048]{1,0:T(8,128)(2,1)}, u32[]{:S(2)}) copy-start(bf16[512,2048]{1,0:T(8,128)(2,1)} %param.26) | copy-start | bytes 6291460
  6.5 77.9 %all-gather.4.cloned.1.call-start = ((), (), s32[]{:S(2)}) async-start(), calls=%async_computation.1 | async-start | bytes 3932160 | tf_op jit(solution)/shard_map/all_gather | solution.py:108
  58.5 77.2 %all-gather.6.cloned.1.call-start = ((), (), s32[]{:S(2)}) async-start(), calls=%async_computation.2 | async-start | bytes 2359296 | tf_op jit(solution)/shard_map/all_gather | solution.py:125
  63.8 248.7 %all-gather.8.cloned.1.call-start = ((), (), s32[]{:S(2)}) async-start(), calls=%async_computation.3 | async-start | bytes 14155776 | tf_op jit(solution)/shard_map/all_gather | solution.py:133
  93.2 1.4 copy-start.4
  96.2 452.7 %reduce-scatter.2.cloned.1.call-start = ((), (), s32[]{:S(2)}) async-start(), calls=%async_computation.4 | async-start | bytes 3932160 | tf_op jit(solution)/shard_map/reduce_scatter | solution.py:143
  146.5 3.1 copy-start.3
  146.5 3.1 copy-start.9
  155.8 8.2 %copy-start.7 = (bf16[1024,512]{0,1:T(8,128)(2,1)S(1)}, bf16[1024,512]{0,1:T(8,128)(2,1)}, u32[]{:S(2)}) copy-start(bf16[1024,512]{0,1:T(8,128)(2,1)} %copy.41) | copy-start | bytes 3145732
  312.6 193.9 %copy-start.10 = (f32[4]{0:T(128)S(1)}, f32[4]{0:T(128)}, u32[]{:S(2)}) copy-start(f32[4]{0:T(128)} %param.27) | copy-start | bytes 52
  312.6 196.2 %copy-start.11 = (f32[128]{0:T(128)S(1)}, f32[128]{0:T(128)}, u32[]{:S(2)}) copy-start(f32[128]{0:T(128)} %param.29) | copy-start | bytes 1540
  330.6 5.8 %copy-start.1 = (bf16[1024,512]{0,1:T(8,128)(2,1)S(1)}, bf16[1024,512]{0,1:T(8,128)(2,1)}, u32[]{:S(2)}) copy-start(bf16[1024,512]{0,1:T(8,128)(2,1)} %get-tuple-element.220) | copy-start | bytes 3145732 | tf_op jit(solution)/shard_map/while
  330.6 5.8 %copy-start.5 = (f32[768,4,128]{0,2,1:T(8,128)S(1)}, f32[768,4,128]{0,2,1:T(8,128)}, u32[]{:S(2)}) copy-start(f32[768,4,128]{0,2,1:T(8,128)} %get-tuple-element.238) | copy-start | bytes 4718596 | tf_op jit(solution)/shard_map/while
  339.7 5.2 copy-start.6
  363.0 5.8 %copy-start.1 = (bf16[1024,512]{0,1:T(8,128)(2,1)S(1)}, bf16[1024,512]{0,1:T(8,128)(2,1)}, u32[]{:S(2)}) copy-start(bf16[1024,512]{0,1:T(8,128)(2,1)} %get-tuple-element.220) | copy-start | bytes 3145732 | tf_op jit(solution)/shard_map/while
  363.0 5.8 %copy-start.5 = (f32[768,4,128]{0,2,1:T(8,128)S(1)}, f32[768,4,128]{0,2,1:T(8,128)}, u32[]{:S(2)}) copy-start(f32[768,4,128]{0,2,1:T(8,128)} %get-tuple-element.238) | copy-start | bytes 4718596 | tf_op jit(solution)/shard_map/while
  372.0 5.2 copy-start.6
  395.3 5.8 %copy-start.1 = (bf16[1024,512]{0,1:T(8,128)(2,1)S(1)}, bf16[1024,512]{0,1:T(8,128)(2,1)}, u32[]{:S(2)}) copy-start(bf16[1024,512]{0,1:T(8,128)(2,1)} %get-tuple-element.220) | copy-start | bytes 3145732 | tf_op jit(solution)/shard_map/while
  395.3 5.8 %copy-start.5 = (f32[768,4,128]{0,2,1:T(8,128)S(1)}, f32[768,4,128]{0,2,1:T(8,128)}, u32[]{:S(2)}) copy-start(f32[768,4,128]{0,2,1:T(8,128)} %get-tuple-element.238) | copy-start | bytes 4718596 | tf_op jit(solution)/shard_map/while
  404.3 5.2 copy-start.6
  427.6 5.8 %copy-start.1 = (bf16[1024,512]{0,1:T(8,128)(2,1)S(1)}, bf16[1024,512]{0,1:T(8,128)(2,1)}, u32[]{:S(2)}) copy-start(bf16[1024,512]{0,1:T(8,128)(2,1)} %get-tuple-element.220) | copy-start | bytes 3145732 | tf_op jit(solution)/shard_map/while
  427.6 5.8 %copy-start.5 = (f32[768,4,128]{0,2,1:T(8,128)S(1)}, f32[768,4,128]{0,2,1:T(8,128)}, u32[]{:S(2)}) copy-start(f32[768,4,128]{0,2,1:T(8,128)} %get-tuple-element.238) | copy-start | bytes 4718596 | tf_op jit(solution)/shard_map/while
  436.6 5.2 copy-start.6
  459.9 5.8 %copy-start.1 = (bf16[1024,512]{0,1:T(8,128)(2,1)S(1)}, bf16[1024,512]{0,1:T(8,128)(2,1)}, u32[]{:S(2)}) copy-start(bf16[1024,512]{0,1:T(8,128)(2,1)} %get-tuple-element.220) | copy-start | bytes 3145732 | tf_op jit(solution)/shard_map/while
  459.9 5.8 %copy-start.5 = (f32[768,4,128]{0,2,1:T(8,128)S(1)}, f32[768,4,128]{0,2,1:T(8,128)}, u32[]{:S(2)}) copy-start(f32[768,4,128]{0,2,1:T(8,128)} %get-tuple-element.238) | copy-start | bytes 4718596 | tf_op jit(solution)/shard_map/while
  468.9 5.2 copy-start.6
  492.2 5.8 %copy-start.1 = (bf16[1024,512]{0,1:T(8,128)(2,1)S(1)}, bf16[1024,512]{0,1:T(8,128)(2,1)}, u32[]{:S(2)}) copy-start(bf16[1024,512]{0,1:T(8,128)(2,1)} %get-tuple-element.220) | copy-start | bytes 3145732 | tf_op jit(solution)/shard_map/while
  492.2 5.8 %copy-start.5 = (f32[768,4,128]{0,2,1:T(8,128)S(1)}, f32[768,4,128]{0,2,1:T(8,128)}, u32[]{:S(2)}) copy-start(f32[768,4,128]{0,2,1:T(8,128)} %get-tuple-element.238) | copy-start | bytes 4718596 | tf_op jit(solution)/shard_map/while
  501.3 5.2 copy-start.6
  509.1 39.8 %copy-start.2 = (bf16[192,2048]{1,0:T(8,128)(2,1)S(1)}, bf16[192,2048]{1,0:T(8,128)(2,1)}, u32[]{:S(2)}) copy-start(bf16[192,2048]{1,0:T(8,128)(2,1)} %param.16) | copy-start | bytes 2359300
  509.1 39.8 %copy-start.8 = (f32[1,1,2048]{2,0,1:T(1,128)S(1)}, f32[1,1,2048]{2,0,1:T(1,128)}, u32[]{:S(2)}) copy-start(f32[1,1,2048]{2,0,1:T(1,128)} %get-tuple-element.125) | copy-start | bytes 24580
Sparse Core Ops, SparseCore 0:
  58.6 25.7 all-gather.3
  86.6 49.0 all-gather.5
  137.9 174.6 all-gather.7
  512.8 36.0 reduce-scatter.1
where the time goes:
time: 559 us; the launch traced here: 558 us
  waiting for transfers between devices  232 us (42%)
  matrix products  145 us (26%)
  local copies, waits for them, and re-layouts  72.2 us (13%)
  other arithmetic  49.9 us (9%)
  blocking collectives  44 us (8%)
  between operations  13.3 us (2%)
    all_gather x1, waiting for transfers between devices, per_device(): portion = lax.all_gather(latent_kv, 'sp', axis=0, tiled=True)  136 us
    dot_general x14, matrix products, absorb(): jnp.einsum('hqk,khd->qhd', raised.astype(jnp.bfloat16), value_rows, prefe...  66.5 us
    dot_general x14, matrix products, absorb(): jnp.einsum('qhd,khd->hqk', queries[:, :, which_map], key_rows[:, :, which...  59 us
    dynamic_slice x12, local copies, waits for them, and re-layouts, absorb_rows(): running, unused = lax.scan(advance, running, (stacked, flag_blocks))  42.2 us
    all_gather x1, waiting for transfers between devices, per_device(): every_context = lax.all_gather(context_kv, 'sp', axis=0, tiled=True)  39.3 us
    reduce_sum x7, other arithmetic, absorb(): weight = weight * faded + jnp.sum(raised, axis=2)  39 us
    psum x1, blocking collectives, per_device(): summed = lax.psum(partials, 'sp')  38.8 us
    reduce_scatter x1, waiting for transfers between devices, per_device(): lax.psum_scatter(jnp.dot(flattened, w_out, preferred_element_type=jnp.flo...  36.2 us
  transfers between devices with their start and end apart: 4, of which 4 were waited for; matrix products, arithmetic and copies ran while one was open for 10% of the time, Pallas kernels for 0%

commit v1 on v0

v1 whole, which is shorter than its diff:
```python
import functools, math
import jax, jax.numpy as jnp
from jax import lax
from jax.sharding import PartitionSpec as P
from jax.experimental import pallas as pl
from jax.experimental.pallas import tpu as pltpu
EPS=1e-6
LOG2E=math.log2(math.e)

def attn_kernel(cfg, lam_ref, bias_ref, q_ref, kv_ref, gain_ref, o_ref, vt_ref, m_s, l_s, a_s):
    blocks, rows, ctx, hd = cfg
    i = pl.program_id(1)
    c = hd ** -0.5 * LOG2E
    @pl.when(i == 0)
    def _():
        def tr(b, _):
            vt_ref[b] = kv_ref[b, 1].T
            return 0
        lax.fori_loop(0, blocks, tr, 0)
    q = q_ref[0]
    lane = lax.broadcasted_iota(jnp.int32, q.shape, 1)
    zero = jnp.zeros_like(q)
    qs = (jnp.where(lane < hd, q, zero), jnp.where(lane < hd, zero, q))
    m_s[...] = jnp.full_like(m_s, -1e30)
    l_s[...] = jnp.zeros_like(l_s)
    a_s[...] = jnp.zeros_like(a_s)
    bias = bias_ref[0, 0] * LOG2E
    def body(b, _):
        k = kv_ref[b, 0]
        vt = vt_ref[b]
        for m in range(2):
            s = lax.dot_general(k, qs[m], (((1,), (1,)), ((), ())), preferred_element_type=jnp.float32) * c
            s = jnp.concatenate([s[:ctx] + bias, s[ctx:]], axis=0)
            old = m_s[m]
            new = jnp.maximum(old, jnp.max(s, axis=0, keepdims=True))
            fade = jnp.exp2(old - new)
            p = jnp.exp2(s - new)
            l_s[m] = l_s[m] * fade + jnp.sum(p, axis=0, keepdims=True)
            a_s[m] = a_s[m] * fade + jnp.dot(vt, p.astype(jnp.bfloat16), preferred_element_type=jnp.float32)
            m_s[m] = new
        return 0
    lax.fori_loop(0, blocks, body, 0)
    mixed = a_s[0] / l_s[0] - lam_ref[0, 0] * (a_s[1] / l_s[1])
    normed = mixed * lax.rsqrt(jnp.mean(mixed * mixed, axis=0, keepdims=True) + EPS)
    o_ref[0] = (normed.T * gain_ref[...]).astype(jnp.bfloat16)

def attn(q, kv, ctx, lam, bias, gain, bq=256):
    heads, T, w = q.shape
    B, _, R, _ = kv.shape
    return pl.pallas_call(
        functools.partial(attn_kernel, (B, R, ctx, w // 2)),
        grid=(1, T // bq),
        in_specs=[pl.BlockSpec(memory_space=pltpu.SMEM), pl.BlockSpec(memory_space=pltpu.SMEM),
                  pl.BlockSpec((1, bq, w), lambda h, i: (h, i, 0)),
                  pl.BlockSpec((B, 2, R, w), lambda h, i: (0, 0, 0, 0)),
                  pl.BlockSpec((1, w), lambda h, i: (0, 0))],
        out_specs=pl.BlockSpec((1, bq, w), lambda h, i: (h, i, 0)),
        out_shape=jax.ShapeDtypeStruct((heads, T, w), jnp.bfloat16),
        scratch_shapes=[pltpu.VMEM((B, w, R), jnp.bfloat16), pltpu.VMEM((2, 1, bq), jnp.float32),
                        pltpu.VMEM((2, 1, bq), jnp.float32), pltpu.VMEM((2, w, bq), jnp.float32)],
    )(lam, bias, q, kv, gain)


def modulated(inputs, norm_scale, offset_vec, scale_vec):
    rows_float = inputs.astype(jnp.float32)
    normal = rows_float * lax.rsqrt(jnp.mean(rows_float * rows_float, axis=-1, keepdims=True) + EPS)
    return (normal * norm_scale * (1.0 + scale_vec) + offset_vec).astype(jnp.bfloat16)


def per_device(sizes, latent, context, conditioning, norm_gain, mod_shift, mod_scale, mod_gate, w_query, w_key, w_value, w_out, lambdas, context_bias, head_gain):
    n_sp, n_tp = sizes
    width = head_gain.shape[0]
    heads = lambdas.shape[0]
    split = math.gcd(heads, n_sp)
    rest = n_sp // split
    own = heads // split
    exchange = [[z * rest + x for z in range(split)] for x in range(rest)]
    gather = [[z * rest + x for x in range(rest)] for z in range(split)]
    place = lax.axis_index("sp")

    every_row = lax.all_gather(latent, "tp", axis=0, tiled=True)
    rows_sp = mod_shift.shape[0]
    cond_rows = lax.dynamic_slice_in_dim(conditioning, place * rows_sp, rows_sp, 1)
    activated = jax.nn.silu(cond_rows).astype(jnp.bfloat16)
    partials = jnp.stack(
        [jnp.dot(activated, matrix, preferred_element_type=jnp.float32) for matrix in (mod_shift, mod_scale, mod_gate)],
        axis=1,
    )
    parts = lax.all_gather(partials, ("sp", "tp"), axis=0, tiled=False)
    parts = parts.reshape((n_sp, n_tp) + partials.shape).sum(axis=0)
    modulation = jnp.moveaxis(parts, 0, 2).reshape(2, 3, -1)

    context_rows = modulated(context, norm_gain, modulation[1, 0], modulation[1, 1])
    rows = modulated(every_row, norm_gain, modulation[0, 0], modulation[0, 1])
    key_value = jnp.concatenate([w_key, w_value], axis=1)
    dot = functools.partial(jnp.dot, preferred_element_type=jnp.float32)
    tokens, ctx = rows.shape[0], context_rows.shape[0]
    both = jnp.concatenate([context_rows, rows], axis=0)
    count = tokens + ctx

    def by_head(matrix, columns):
        product = dot(matrix, columns).astype(jnp.bfloat16)
        return jnp.moveaxis(product.reshape(matrix.shape[0], heads, width), 1, 0)

    payload = jnp.concatenate([by_head(rows, w_query), by_head(both, w_key), by_head(both, w_value)], axis=1)
    got = lax.all_to_all(payload, "sp", 0, 0, axis_index_groups=exchange, tiled=True)
    got = got.reshape(split, own, tokens + 2 * count, width)
    queries = jnp.moveaxis(got[:, :, :tokens], 1, 0).reshape(own, split * tokens, width)
    kv = got[:, :, tokens:].reshape(split, own, 2, count, width)
    if rest > 1:
        kv = lax.all_gather(kv, "sp", axis=0, axis_index_groups=gather, tiled=True)
    start = (place // rest) * own
    lams = lax.dynamic_slice_in_dim(lambdas, start, own).reshape(own, 1)
    biases = lax.dynamic_slice_in_dim(context_bias, start, own).reshape(own, 1)
    block = max(b for b in range(8, 1025, 8) if split * tokens % b == 0)
    outs = [
        attn(queries[h : h + 1], kv[:, h], ctx, lams[h : h + 1], biases[h : h + 1], head_gain.reshape(1, width), block)
        for h in range(own)
    ]
    normed = jnp.concatenate(outs, axis=0).reshape(own, split, tokens, width)
    back = lax.all_to_all(jnp.moveaxis(normed, 1, 0), "sp", 0, 0, axis_index_groups=exchange, tiled=True)
    flattened = jnp.moveaxis(back.reshape(heads, tokens, width), 0, 1).reshape(tokens, heads * width)
    attended = lax.psum_scatter(dot(flattened, w_out).astype(jnp.bfloat16), "tp", scatter_dimension=0, tiled=True)
    return (latent.astype(jnp.float32) + modulation[0, 2] * attended.astype(jnp.float32)).astype(jnp.bfloat16)


def solution(mesh):
    sizes = (mesh.shape["sp"], mesh.shape["tp"])
    return jax.shard_map(
        functools.partial(per_device, sizes),
        mesh=mesh,
        in_specs=(P(("sp", "tp"), None), P("sp", None), P(), P(), P("sp", "tp"), P("sp", "tp"), P("sp", "tp"),
                  P(None, "tp"), P(None, "tp"), P(None, "tp"), P("tp", None), P("tp"), P("tp"), P()),
        out_specs=P(("sp", "tp"), None),
        check_vma=False,
    )
```

time: 559 us -> 354 us (0.63)
  waiting for transfers between devices: 232 us -> 81.5 us
  matrix products: 145 us -> 21.3 us
  blocking collectives: 44 us -> 132 us
  Pallas kernels: 0 us -> 82.2 us
  local copies, waits for them, and re-layouts: 72.2 us -> 14.2 us
  other arithmetic: 49.9 us -> 8.47 us
    all_gather x3 -> x2, waiting for transfers between devices: 196 us -> 44.6 us  [the longest x1 44.6 us: per_device(): kv = lax.all_gather(kv, 'sp', axis=0, axis_index_groups=gather, tiled=True)]
    dot_general x31 -> x4, matrix products: 142 us -> 18 us  [the longest x3 14.5 us: by_head(): product = dot(matrix, columns).astype(jnp.bfloat16)]
    all_to_all x0 -> x2, blocking collectives: none -> 87 us  [the longest x1 62.7 us: per_device(): lax.all_to_all(payload, 'sp', 0, 0, axis_index_groups=exchange, tiled=True)]
    pallas_call x0 -> x1, Pallas kernels: none -> 82.2 us  [attn(): pl.pallas_call(functools.partial(attn_kernel, (B, R, ctx, w // 2)), grid=...]
    reduce_sum x8 -> x1, other arithmetic: 41.3 us -> 0.1 us  [per_device(): parts = parts.reshape((n_sp, n_tp) + partials.shape).sum(axis=0)]
    dynamic_slice x12 -> x2, local copies, waits for them, and re-layouts: 42.2 us -> 1.3 us  [the longest x1 0.66 us: per_device(): lams = lax.dynamic_slice_in_dim(lambdas, start, own).reshape(own, 1)]
    all_gather x1, blocking collectives: 5.2 us -> 45.1 us  [per_device(): parts = lax.all_gather(partials, ('sp', 'tp'), axis=0, tiled=False)]
    psum x1 -> x0, blocking collectives: 38.8 us -> none  [per_device(): summed = lax.psum(partials, 'sp')]
  transfers between devices with their start and end apart: 4 -> 3, of which waited for: 4 -> 2; matrix products, arithmetic and copies ran while one was open for 10% -> 2% of each run, Pallas kernels for 0% -> 0%
where the time goes in v1:
time: 354 us; the launch traced here: 353 us
  blocking collectives  132 us (37%)
  Pallas kernels  82.2 us (23%)
  waiting for transfers between devices  81.5 us (23%)
  matrix products  21.3 us (6%)
  local copies, waits for them, and re-layouts  14.2 us (4%)
  between operations  13.3 us (4%)
  other arithmetic  8.47 us (2%)
    pallas_call x1, Pallas kernels, attn(): pl.pallas_call(functools.partial(attn_kernel, (B, R, ctx, w // 2)), grid=...  82.2 us
    all_to_all x1, blocking collectives, per_device(): lax.all_to_all(payload, 'sp', 0, 0, axis_index_groups=exchange, tiled=True)  62.7 us
    all_gather x1, blocking collectives, per_device(): parts = lax.all_gather(partials, ('sp', 'tp'), axis=0, tiled=False)  45.1 us
    all_gather x1, waiting for transfers between devices, per_device(): kv = lax.all_gather(kv, 'sp', axis=0, axis_index_groups=gather, tiled=True)  44.6 us
    reduce_scatter x1, waiting for transfers between devices, per_device(): lax.psum_scatter(dot(flattened, w_out).astype(jnp.bfloat16), 'tp', scatte...  36.2 us
    all_to_all x1, blocking collectives, per_device(): lax.all_to_all(jnp.moveaxis(normed, 1, 0), 'sp', 0, 0, axis_index_groups=...  24.3 us
    dot_general x3, matrix products, by_head(): product = dot(matrix, columns).astype(jnp.bfloat16)  14.5 us
  transfers between devices with their start and end apart: 3, of which 2 were waited for; matrix products, arithmetic and copies ran while one was open for 2% of the time, Pallas kernels for 0%

profile of v1, /device:TPU:0, one launch (start us, length us, event | category | flops | bytes accessed | tf_op | source)
XLA Modules:
  0.0 353.4 jit_solution(15652451665680389074)
XLA Ops:
  6.5 0.0 copy-start
  6.5 0.0 copy-start.5
  6.5 0.0 copy-start.6
  6.5 0.0 all-gather.4.cloned.1.call-start
  6.5 0.7 all-gather.4.cloned.1.call-update
  7.3 0.0 all-gather.6.cloned.1.call-start
  7.3 1.1 convolution_bitcast_fusion
  8.4 1.1 convolution_bitcast_fusion.1
  9.6 1.1 convolution_bitcast_fusion.2
  10.7 45.1 %all-gather = f32[64,3,512]{2,1,0:T(4,128)S(1)} all-gather(f32[2,3,512]{2,1,0:T(4,128)S(1)} %copy.22), channel_id=2, replica_groups=mesh['sp'=8,'tp'=4] {'sp','tp'}, dimensions={0}, use_global_device_ids=true | all-gather | bytes 405504 | tf_op jit(solution)/shard_map/all_gather | solution.py:89
  55.8 0.1 reduce_sum.27
  55.9 0.0 copy-done.5
  55.9 0.2 fusion.9
  56.2 0.0 copy-done.6
  56.2 0.3 fusion.13
  56.5 0.0 all-gather.4.cloned.1.call-done
  56.5 0.0 copy-start.1
  56.5 2.7 fusion
  59.2 0.1 copy-done.1
  59.3 0.0 copy-start.7
  59.3 1.2 fusion.4
  60.6 0.3 copy-done.7
  60.9 0.0 copy-start.4
  60.9 3.4 fusion.8
  64.3 0.0 copy-done.4
  64.3 1.5 copy.26
  65.9 5.8 %fusion.7 = bf16[896,512]{0,1:T(8,128)(2,1)} fusion(bf16[2048,512]{1,0:T(8,128)(2,1)} %param.22, bf16[768,2048]{1,0:T(8,128)(2,1)} %copy-done.4, bf16[128,2048]{1,0:T(8,128)(2,1)S(1)} %fusion.13), kind=kOutput, calls=%fused_computation.13 | convolution fusion | flops 1886846976 | bytes 6684672 | tf_op jit(solution)/shard_map/dot_general | solution.py:102
  71.7 2.2 copy.25
  73.9 5.3 %convolution_convert_fusion.1 = bf16[768,512]{0,1:T(8,128)(2,1)} fusion(bf16[768,2048]{1,0:T(8,128)(2,1)} %copy-done.4, bf16[2048,512]{1,0:T(8,128)(2,1)} %param.21), kind=kOutput, calls=%fused_computation.15 | convolution fusion | flops 1611005952 | bytes 6029312 | tf_op jit(solution)/shard_map/dot_general | solution.py:102
  79.2 2.3 copy.24
  81.5 1.6 pad_maximum_fusion.1
  83.1 62.7 %all_to_all.10 = bf16[4,2560,128]{2,1,0:T(8,128)(2,1)S(1)} all-to-all(bf16[4,2560,128]{2,1,0:T(8,128)(2,1)S(1)} %pad_maximum_fusion.1), channel_id=1, replica_groups={{0,8,16,24},{4,12,20,28},{1,9,17,25},{5,13,21,29},{2,10,18,26},{6,14,22..., dimensions={0} | all-to-all | bytes 5242880 | tf_op jit(solution)/shard_map/all_to_all | solution.py:106
  145.8 0.0 copy-start.2
  145.8 0.0 copy-start.8
  145.8 0.0 copy-start.9
  145.8 1.5 copy-done.2
  147.3 1.4 slice.34
  148.6 0.0 all-gather.6.cloned.1.call-update
  148.7 0.2 reduce-scatter.2.cloned.1.call-start
  148.9 0.0 copy-done.8
  148.9 0.7 dynamic_slice.10
  149.6 0.0 copy-done.9
  149.6 0.6 dynamic_slice.11
  150.2 2.1 slice.33
  152.3 44.6 %all-gather.6.cloned.1.call-done = bf16[8,1,2,896,128]{4,3,2,1,0:T(8,128)(2,1)} async-done(((bf16[4,1,2,896,128]{4,3,2,1,0:T(8,128)(2,1)}), bf16[8,1,2,896,128]{4,3,2,1,0:T(8,128)(2,1)}) %all-gather.6.cloned.1.call-update) | async-done | bytes 3670032 | tf_op jit(solution)/shard_map/all_gather | solution.py:111
  196.9 82.2 %shard_map.136 = bf16[1,3072,128]{2,1,0:T(8,128)(2,1)} custom-call(f32[1,1]{1,0:T(1,128)} %bitcast.7.lam_ref, f32[1,1]{1,0:T(1,128)} %bitcast.8.bias_ref, bf16[1,3072,128]{2,1,0:T(8,128)(2,1)} %bitcast.49, bf16[8,2,896,128]{3,2,1,0:T(8,128)(2,1)} %bitcast.48, f32[1,128]{1,0:T(1,128)} %bitcast.63), custom_call_target="tpu_custom_call" | custom-call | tf_op jit(solution)/shard_map/pallas_call | solution.py:50
  279.1 1.4 copy.27
  280.5 24.3 %all_to_all.11 = bf16[4,1,768,128]{2,3,1,0:T(8,128)(2,1)S(1)} all-to-all(bf16[4,1,768,128]{2,3,1,0:T(8,128)(2,1)S(1)} %copy.27), channel_id=1, replica_groups={{0,8,16,24},{4,12,20,28},{1,9,17,25},{5,13,21,29},{2,10,18,26},{6,14,22..., dimensions={0} | all-to-all | bytes 1572864 | tf_op jit(solution)/shard_map/all_to_all | solution.py:121
  304.8 0.0 copy-done
  304.8 3.5 convolution_convert_fusion
  308.3 0.0 copy-start.3
  308.3 0.0 reduce-scatter.2.cloned.1.call-update
  308.3 36.2 %reduce-scatter.2.cloned.1.call-done = bf16[192,2048]{1,0:T(8,128)(2,1)} async-done(((bf16[768,2048]{1,0:T(8,128)(2,1)}), bf16[192,2048]{1,0:T(8,128)(2,1)}) %reduce-scatter.2.cloned.1.call-update) | async-done | bytes 786448 | tf_op jit(solution)/shard_map/reduce_scatter | solution.py:123
  344.5 0.0 copy-done.3
  344.5 2.3 add_convert_fusion
  (6 shorter events, 0.1 us)
Async XLA Ops:
  6.5 298.3 %copy-start = (bf16[512,2048]{1,0:T(8,128)(2,1)S(1)}, bf16[512,2048]{1,0:T(8,128)(2,1)}, u32[]{:S(2)}) copy-start(bf16[512,2048]{1,0:T(8,128)(2,1)} %param.24) | copy-start | bytes 6291460
  6.5 49.4 %copy-start.5 = (bf16[128,2048]{1,0:T(8,128)(2,1)S(1)}, bf16[128,2048]{1,0:T(8,128)(2,1)}, u32[]{:S(2)}) copy-start(bf16[128,2048]{1,0:T(8,128)(2,1)} %param.15) | copy-start | bytes 1572868
  6.5 49.6 %copy-start.6 = (f32[2048]{0:T(1024)S(1)}, f32[2048]{0:T(1024)}, u32[]{:S(2)}) copy-start(f32[2048]{0:T(1024)} %param.17) | copy-start | bytes 24580
  6.5 49.9 %all-gather.4.cloned.1.call-start = ((), (), s32[]{:S(2)}) async-start(), calls=%async_computation.3 | async-start | bytes 3932160 | tf_op jit(solution)/shard_map/all_gather | solution.py:81
  7.3 189.6 %all-gather.6.cloned.1.call-start = ((), (), s32[]{:S(2)}) async-start(), calls=%async_computation.4 | async-start | bytes 5505024 | tf_op jit(solution)/shard_map/all_gather | solution.py:111
  56.5 2.8 copy-start.1
  59.3 1.6 copy-start.7
  60.9 3.4 copy-start.4
  145.8 1.5 copy-start.2
  145.8 3.1 copy-start.8
  145.8 3.8 %copy-start.9 = (f32[4]{0:T(128)S(1)}, f32[4]{0:T(128)}, u32[]{:S(2)}) copy-start(f32[4]{0:T(128)} %param.26) | copy-start | bytes 52
  148.7 195.9 %reduce-scatter.2.cloned.1.call-start = ((), (), s32[]{:S(2)}) async-start(), calls=%async_computation.5 | async-start | bytes 3932160 | tf_op jit(solution)/shard_map/reduce_scatter | solution.py:123
  308.3 36.2 %copy-start.3 = (bf16[192,2048]{1,0:T(8,128)(2,1)S(1)}, bf16[192,2048]{1,0:T(8,128)(2,1)}, u32[]{:S(2)}) copy-start(bf16[192,2048]{1,0:T(8,128)(2,1)} %param.14) | copy-start | bytes 2359300
Sparse Core Ops, SparseCore 0:
  8.9 34.2 all-gather.3
  148.8 48.0 all-gather.5
  308.4 36.0 reduce-scatter.1

commit v2 on v1

v2 whole, which is shorter than its diff:
```python
import functools
import math
import jax
import jax.numpy as jnp
from jax import lax
from jax.experimental import pallas as pl
from jax.experimental.pallas import tpu as pltpu
from jax.sharding import PartitionSpec as P

EPS = 1e-6
LOG2E = math.log2(math.e)


def attn_kernel(cfg, lam_ref, bias_ref, q_ref, k_ref, v_ref, gain_ref, o_ref, vt_ref, m_s, l_s, a_s):
    blocks, rows, ctx, hd = cfg
    h, i = pl.program_id(0), pl.program_id(1)
    c = hd**-0.5 * LOG2E

    @pl.when(i == 0)
    def _():
        def turn(b, _):
            vt_ref[b] = v_ref[b].T
            return 0

        lax.fori_loop(0, blocks, turn, 0)

    q = q_ref[...]
    lane = lax.broadcasted_iota(jnp.int32, q.shape, 1)
    zero = jnp.zeros_like(q)
    qs = (jnp.where(lane < hd, q, zero), jnp.where(lane < hd, zero, q))
    m_s[...] = jnp.full_like(m_s, -1e30)
    l_s[...] = jnp.zeros_like(l_s)
    a_s[...] = jnp.zeros_like(a_s)
    bias = bias_ref[h] * LOG2E

    def body(b, _):
        k = k_ref[b]
        vt = vt_ref[b]
        for m in range(2):
            s = lax.dot_general(k, qs[m], (((1,), (1,)), ((), ())), preferred_element_type=jnp.float32) * c
            s = jnp.concatenate([s[:ctx] + bias, s[ctx:]], axis=0)
            old = m_s[m]
            new = jnp.maximum(old, jnp.max(s, axis=0, keepdims=True))
            fade = jnp.exp2(old - new)
            p = jnp.exp2(s - new)
            l_s[m] = l_s[m] * fade + jnp.sum(p, axis=0, keepdims=True)
            a_s[m] = a_s[m] * fade + jnp.dot(vt, p.astype(jnp.bfloat16), preferred_element_type=jnp.float32)
            m_s[m] = new
        return 0

    lax.fori_loop(0, blocks, body, 0)
    mixed = a_s[0] / l_s[0] - lam_ref[h] * (a_s[1] / l_s[1])
    normed = mixed * lax.rsqrt(jnp.mean(mixed * mixed, axis=0, keepdims=True) + EPS)
    o_ref[...] = (normed.T * gain_ref[...]).astype(jnp.bfloat16)


def attn(q, k, v, ctx, lam, bias, gain, bq):
    T, columns = q.shape
    w = gain.shape[1]
    heads = columns // w
    B, R, _ = k.shape
    ops = 8 * T * B * R * w * heads
    return pl.pallas_call(
        functools.partial(attn_kernel, (B, R, ctx, w // 2)),
        grid=(heads, T // bq),
        in_specs=[
            pl.BlockSpec(memory_space=pltpu.SMEM),
            pl.BlockSpec(memory_space=pltpu.SMEM),
            pl.BlockSpec((bq, w), lambda h, i: (i, h)),
            pl.BlockSpec((B, R, w), lambda h, i: (0, 0, h)),
            pl.BlockSpec((B, R, w), lambda h, i: (0, 0, h)),
            pl.BlockSpec((1, w), lambda h, i: (0, 0)),
        ],
        out_specs=pl.BlockSpec((bq, w), lambda h, i: (i, h)),
        out_shape=jax.ShapeDtypeStruct((T, columns), jnp.bfloat16),
        scratch_shapes=[
            pltpu.VMEM((B, w, R), jnp.bfloat16),
            pltpu.VMEM((2, 1, bq), jnp.float32),
            pltpu.VMEM((2, 1, bq), jnp.float32),
            pltpu.VMEM((2, w, bq), jnp.float32),
        ],
        cost_estimate=pl.CostEstimate(flops=4 * ops, bytes_accessed=2 * T * columns, transcendentals=2 * T * B * R * heads),
    )(lam, bias, q, k, v, gain)


def greet(peers):
    barrier = pltpu.get_barrier_semaphore()
    for peer in peers:
        pl.semaphore_signal(barrier, inc=1, device_id=peer, device_id_type=pl.DeviceIdType.MESH)
    pl.semaphore_wait(barrier, len(peers))


def remote(source, target, send, recv, peer):
    return pltpu.make_async_remote_copy(
        src_ref=source, dst_ref=target, send_sem=send, recv_sem=recv, device_id=peer, device_id_type=pl.DeviceIdType.MESH
    )


def exchange_kernel(split, rest, wide, q_ref, k_ref, v_ref, qo, ko, vo, zs, zr, xs, xr, ls):
    place = lax.axis_index("sp")
    z, x = place // rest, lax.rem(place, rest)
    z_peer = [lax.rem(z + d, split) for d in range(split)]
    x_peer = [lax.rem(x + d, rest) for d in range(rest)]
    greet([{"sp": z_peer[d] * rest + x} for d in range(1, split)] + [{"sp": z * rest + x_peer[d]} for d in range(1, rest)])

    def cols(index):
        return pl.ds(pl.multiple_of(index * wide, wide), wide)

    sends, lands = [], []
    pairs = ((k_ref, ko), (v_ref, vo))
    for d in range(1, rest):
        for a, (src, out) in enumerate(pairs):
            sends.append(remote(src.at[:, cols(z)], out.at[place], xs.at[0, d, a], xr.at[0, d, a], {"sp": z * rest + x_peer[d]}))
            sends[-1].start()
    first = {}
    for a, (src, out) in enumerate(pairs + ((q_ref, qo),)):
        for d in range(1, split):
            mine = out.at[place] if a < 2 else out.at[z]
            first[d, a] = remote(src.at[:, cols(z_peer[d])], mine, zs.at[d, a], zr.at[d, a], {"sp": z_peer[d] * rest + x})
            first[d, a].start()
    local = []
    for a, (src, out) in enumerate(pairs + ((q_ref, qo),)):
        mine = out.at[place] if a < 2 else out.at[z]
        local.append(pltpu.make_async_copy(src.at[:, cols(z)], mine, ls.at[a]))
        local[-1].start()
    for a, (src, out) in enumerate(pairs):
        for d in range(1, split):
            first[d, a].wait_recv()
            slot = lax.rem(z + split - d, split) * rest + x
            for e in range(1, rest):
                sends.append(remote(out.at[slot], out.at[slot], xs.at[d, e, a], xr.at[d, e, a], {"sp": z * rest + x_peer[e]}))
                sends[-1].start()
    for copy in local:
        copy.wait()
    for d in range(1, split):
        first[d, 2].wait_recv()
        for a in range(3):
            first[d, a].wait_send()
    for copy in sends:
        copy.wait()


def exchange(q, k, v, split, rest, wide):
    tokens, count = q.shape[0], k.shape[0]
    dma = pltpu.SemaphoreType.DMA
    vm = pl.BlockSpec(memory_space=pltpu.VMEM)
    return pl.pallas_call(
        functools.partial(exchange_kernel, split, rest, wide),
        in_specs=[vm] * 3,
        out_specs=[vm] * 3,
        out_shape=[
            jax.ShapeDtypeStruct((split, tokens, wide), q.dtype),
            jax.ShapeDtypeStruct((split * rest, count, wide), q.dtype),
            jax.ShapeDtypeStruct((split * rest, count, wide), q.dtype),
        ],
        scratch_shapes=[dma((split, 3)), dma((split, 3)), dma((split, rest, 2)), dma((split, rest, 2)), dma((3,))],
        compiler_params=pltpu.CompilerParams(collective_id=0, has_side_effects=True, vmem_limit_bytes=40 * 2**20),
        cost_estimate=pl.CostEstimate(flops=0, bytes_accessed=80_000_000, transcendentals=0),
    )(q, k, v)


def spread_kernel(split, rest, n_tp, wide, own_rows, o_ref, out_ref, ss, rs, ls):
    place, t = lax.axis_index("sp"), lax.axis_index("tp")
    z, x = place // rest, lax.rem(place, rest)
    offsets = [(d, e) for d in range(split) for e in range(n_tp)]
    peers = {(d, e): (lax.rem(z + d, split), lax.rem(t + e, n_tp)) for d, e in offsets}
    greet([{"sp": peers[o][0] * rest + x, "tp": peers[o][1]} for o in offsets[1:]])
    mine = out_ref.at[:, pl.ds(pl.multiple_of((t * split + z) * wide, wide), wide)]
    copies = []
    for d, e in offsets:
        zp, tp = peers[d, e]
        source = o_ref.at[pl.ds(pl.multiple_of((zp * n_tp + tp) * own_rows, own_rows), own_rows), :]
        if d == 0 and e == 0:
            copies.append(pltpu.make_async_copy(source, mine, ls.at[0]))
        else:
            copies.append(remote(source, mine, ss.at[d, e], rs.at[d, e], {"sp": zp * rest + x, "tp": tp}))
        copies[-1].start()
    for copy in copies:
        copy.wait()


def spread(o, split, rest, n_tp, wide, own_rows):
    dma = pltpu.SemaphoreType.DMA
    vm = pl.BlockSpec(memory_space=pltpu.VMEM)
    return pl.pallas_call(
        functools.partial(spread_kernel, split, rest, n_tp, wide, own_rows),
        in_specs=[vm],
        out_specs=vm,
        out_shape=jax.ShapeDtypeStruct((own_rows, n_tp * split * wide), o.dtype),
        scratch_shapes=[dma((split, n_tp)), dma((split, n_tp)), dma((1,))],
        compiler_params=pltpu.CompilerParams(collective_id=1, has_side_effects=True, vmem_limit_bytes=16 * 2**20),
        cost_estimate=pl.CostEstimate(flops=0, bytes_accessed=20_000_000, transcendentals=0),
    )(o)


def modulated(inputs, norm_scale, offset_vec, scale_vec):
    rows_float = inputs.astype(jnp.float32)
    normal = rows_float * lax.rsqrt(jnp.mean(rows_float * rows_float, axis=-1, keepdims=True) + EPS)
    return (normal * norm_scale * (1.0 + scale_vec) + offset_vec).astype(jnp.bfloat16)


def per_device(sizes, latent, context, conditioning, norm_gain, mod_shift, mod_scale, mod_gate, w_query, w_key, w_value, w_out, lambdas, context_bias, head_gain):
    n_sp, n_tp = sizes
    width = head_gain.shape[0]
    heads = lambdas.shape[0]
    split = math.gcd(heads, n_sp)
    rest = n_sp // split
    own = heads // split
    place = lax.axis_index("sp")

    every_row = lax.all_gather(latent, "tp", axis=0, tiled=True)
    w_out, every_row = lax.optimization_barrier((w_out, every_row))
    w_every = lax.all_gather(w_out, "tp", axis=0, tiled=True)
    rows_sp = mod_shift.shape[0]
    cond_rows = lax.dynamic_slice_in_dim(conditioning, place * rows_sp, rows_sp, 1)
    activated = jax.nn.silu(cond_rows).astype(jnp.bfloat16)
    partials = jnp.stack(
        [jnp.dot(activated, matrix, preferred_element_type=jnp.float32) for matrix in (mod_shift, mod_scale, mod_gate)],
        axis=1,
    )
    parts = lax.all_gather(partials, "sp", axis=0, tiled=False).sum(axis=0)
    modulation = lax.all_gather(parts, "tp", axis=2, tiled=True)

    context_rows = modulated(context, norm_gain, modulation[1, 0], modulation[1, 1])
    rows = modulated(every_row, norm_gain, modulation[0, 0], modulation[0, 1])
    dot = functools.partial(jnp.dot, preferred_element_type=jnp.float32)
    tokens, ctx = rows.shape[0], context_rows.shape[0]
    both = jnp.concatenate([context_rows, rows], axis=0)
    q, k, v = [
        dot(matrix, columns).astype(jnp.bfloat16) for matrix, columns in ((rows, w_query), (both, w_key), (both, w_value))
    ]
    q, k, v = exchange(q, k, v, split, rest, own * width)
    start = (place // rest) * own
    lams = lax.dynamic_slice_in_dim(lambdas, start, own)
    biases = lax.dynamic_slice_in_dim(context_bias, start, own)
    total = split * tokens
    block = max(b for b in range(8, 1025, 8) if total % b == 0)
    normed = attn(q.reshape(total, own * width), k, v, ctx, lams, biases, head_gain.reshape(1, width), block)
    flattened = spread(normed, split, rest, n_tp, own * width, latent.shape[0])
    group = heads * width
    summed = 0.0
    for g in range(n_tp):
        partial = dot(flattened[:, g * group : (g + 1) * group], w_every[g * group : (g + 1) * group])
        summed = summed + lax.reduce_precision(partial, 8, 7)
    attended = lax.reduce_precision(summed, 8, 7)
    return (latent.astype(jnp.float32) + modulation[0, 2] * attended).astype(jnp.bfloat16)


def solution(mesh):
    sizes = (mesh.shape["sp"], mesh.shape["tp"])
    return jax.shard_map(
        functools.partial(per_device, sizes),
        mesh=mesh,
        in_specs=(P(("sp", "tp"), None), P("sp", None), P(), P(), P("sp", "tp"), P("sp", "tp"), P("sp", "tp"),
                  P(None, "tp"), P(None, "tp"), P(None, "tp"), P("tp", None), P("tp"), P("tp"), P()),
        out_specs=P(("sp", "tp"), None),
        check_vma=False,
    )
```

time: 354 us -> 277 us (0.78)
  blocking collectives: 132 us -> 36.1 us
  Pallas kernels: 82.2 us -> 164 us
  waiting for transfers between devices: 81.5 us -> 30.2 us
  local copies, waits for them, and re-layouts: 14.2 us -> 5.82 us
  other arithmetic: 8.47 us -> 4.5 us
    all_to_all x2 -> x0, blocking collectives: 87 us -> none  [the longest x1 62.7 us: per_device(): lax.all_to_all(payload, 'sp', 0, 0, axis_index_groups=exchange, tiled=True)]
    pallas_call x0 -> x2, Pallas kernels: none -> 81.6 us  [the longest x1 60.4 us: exchange(): pl.pallas_call(functools.partial(exchange_kernel, split, rest, wide), in_...]
    all_gather x1, waiting for transfers between devices: 44.6 us -> 0.02 us  [per_device(): w_every = lax.all_gather(w_out, 'tp', axis=0, tiled=True)]
    reduce_scatter x1 -> x0, waiting for transfers between devices: 36.2 us -> none  [per_device(): lax.psum_scatter(dot(flattened, w_out).astype(jnp.bfloat16), 'tp', scatte...]
    all_gather x1, waiting for transfers between devices: 0.02 us -> 29.5 us  [per_device(): every_row = lax.all_gather(latent, 'tp', axis=0, tiled=True)]
    all_gather x1 -> x2, blocking collectives: 45.1 us -> 36.1 us  [the longest x1 30.6 us: per_device(): parts = lax.all_gather(partials, 'sp', axis=0, tiled=False).sum(axis=0)]
    reshape x3 -> x0, local copies, waits for them, and re-layouts: 6.06 us -> none  [by_head(): return jnp.moveaxis(product.reshape(matrix.shape[0], heads, width), 1, 0)]
    dot_general x4 -> x7, matrix products: 18 us -> 15.9 us  [the longest x4 9.98 us: per_device(): dot(flattened[:, g * group:(g + 1) * group], w_every[g * group:(g + 1) *...]
  transfers between devices with their start and end apart: 3 -> 2, of which waited for: 2 -> 1; matrix products, arithmetic and copies ran while one was open for 2% -> 5% of each run, Pallas kernels for 0% -> 60%
where the time goes in v2:
time: 277 us; the launch traced here: 274 us
  Pallas kernels  164 us (59%)
  blocking collectives  36.1 us (13%)
  waiting for transfers between devices  30.2 us (11%)
  matrix products  19.2 us (7%)
  between operations  13.7 us (5%)
  local copies, waits for them, and re-layouts  5.82 us (2%)
  other arithmetic  4.5 us (2%)
    pallas_call x1, Pallas kernels, attn(): pl.pallas_call(functools.partial(attn_kernel, (B, R, ctx, w // 2)), grid=...  82.3 us
    pallas_call x1, Pallas kernels, exchange(): pl.pallas_call(functools.partial(exchange_kernel, split, rest, wide), in_...  60.4 us
    all_gather x1, blocking collectives, per_device(): parts = lax.all_gather(partials, 'sp', axis=0, tiled=False).sum(axis=0)  30.6 us
    all_gather x1, waiting for transfers between devices, per_device(): every_row = lax.all_gather(latent, 'tp', axis=0, tiled=True)  29.5 us
    pallas_call x1, Pallas kernels, spread(): pl.pallas_call(functools.partial(spread_kernel, split, rest, n_tp, wide,...  21.2 us
    dot_general x4, matrix products, per_device(): dot(flattened[:, g * group:(g + 1) * group], w_every[g * group:(g + 1) *...  9.98 us
    dot_general x3, matrix products, per_device(): dot(matrix, columns).astype(jnp.bfloat16)  5.92 us
    all_gather x1, blocking collectives, per_device(): modulation = lax.all_gather(parts, 'tp', axis=2, tiled=True)  5.56 us
  transfers between devices with their start and end apart: 2, of which 1 were waited for; matrix products, arithmetic and copies ran while one was open for 5% of the time, Pallas kernels for 60%

profile of v2, /device:TPU:0, one launch (start us, length us, event | category | flops | bytes accessed | tf_op | source)
XLA Modules:
  0.0 273.5 jit_solution(13275656501665826001)
XLA Ops:
  6.5 0.0 copy-start
  6.5 0.0 copy-start.11
  6.5 0.0 copy-start.12
  6.5 0.0 copy-start.7
  6.5 0.0 all-gather.4.cloned.1.call-start
  6.6 0.7 all-gather.4.cloned.1.call-update
  7.3 0.0 copy-start.8
  7.3 0.0 all-gather.6.cloned.1.call-start
  7.3 1.1 convolution_bitcast_fusion
  8.5 1.1 convolution_bitcast_fusion.1
  9.6 1.1 convolution_bitcast_fusion.2
  10.7 29.5 %all-gather.4.cloned.1.call-done = bf16[768,2048]{1,0:T(8,128)(2,1)} async-done(((bf16[192,2048]{1,0:T(8,128)(2,1)}), bf16[768,2048]{1,0:T(8,128)(2,1)}) %all-gather.4.cloned.1.call-update) | async-done | bytes 3145744 | tf_op jit(solution)/shard_map/all_gather | solution.py:211
  40.2 0.0 all-gather.6.cloned.1.call-update
  40.2 30.6 %all-gather = f32[16,3,512]{2,1,0:T(4,128)S(1)} all-gather(f32[2,3,512]{2,1,0:T(4,128)S(1)} %copy.15), channel_id=2, replica_groups=mesh['sp'=8,'tp'=4] {'sp'}, dimensions={0}, use_global_device_ids=true | all-gather | bytes 110592 | tf_op jit(solution)/shard_map/all_gather | solution.py:221
  70.9 0.0 copy-done.11
  70.9 0.7 dynamic_slice.10.lam_ref
  71.5 0.0 copy-done.12
  71.6 0.6 dynamic_slice.11.bias_ref
  72.1 5.6 %all_gather.17 = f32[2,3,2048]{2,0,1:T(2,128)S(1)} all-gather(f32[2,3,512]{2,0,1:T(2,128)S(1)} %copy.17), channel_id=1, replica_groups=mesh['sp'=8,'tp'=4] {'tp'}, dimensions={2}, use_global_device_ids=true | all-gather | bytes 61440 | tf_op jit(solution)/shard_map/all_gather | solution.py:222
  77.7 0.0 copy-done.7
  77.7 0.2 fusion.20
  77.9 0.0 copy-done.8
  77.9 0.0 copy-start.5
  77.9 0.3 fusion.24
  78.2 2.7 fusion
  81.0 0.0 copy-done.5
  81.0 1.2 fusion.4
  82.2 0.0 copy-done
  82.2 0.0 copy-start.9
  82.2 2.1 fusion.18.k_ref
  84.3 0.0 copy-done.9
  84.3 0.0 copy-start.10
  84.3 2.1 fusion.19.v_ref
  86.4 0.0 copy-done.10
  86.4 1.8 convolution_convert_fusion.q_ref
  88.2 60.4 %shard_map.136 = (bf16[4,768,128]{2,1,0:T(8,128)(2,1)S(1)}, bf16[8,896,128]{2,1,0:T(8,128)(2,1)S(1)}, bf16[8,896,128]{2,1,0:T(8,128)(2,1)S(1)}) custom-call(bf16[768,512]{1,0:T(8,128)(2,1)S(1)} %convolution_convert_fusion.q_ref, bf16[896,512]{1,0:T(8,128)(2,1)S(1)} %fusion.18.k_ref, bf16[896,512]{1,0:T(8,128)(2,1)S(1)} %fusion.19.v_ref), custom_call_target="tpu_custom_call" | custom-call | bytes 80000000 | tf_op jit(solution)/shard_map/pallas_call | solution.py:147
  148.6 0.0 copy-start.2
  148.6 1.3 copy-done.2
  149.9 0.0 copy-start.3
  149.9 1.2 copy-done.3
  151.1 0.0 copy-start.4
  151.1 0.9 copy-done.4
  152.0 82.3 %shard_map.137.o_ref = bf16[3072,128]{1,0:T(8,128)(2,1)} custom-call(f32[1]{0:T(128)} %dynamic_slice.10.lam_ref, f32[1]{0:T(128)} %dynamic_slice.11.bias_ref, bf16[3072,128]{1,0:T(8,128)(2,1)} %bitcast.21, bf16[8,896,128]{2,1,0:T(8,128)(2,1)} %copy-done.2, bf16[8,896,128]{2,1,0:T(8,128)(2,1)} %copy-done.3, f32[1,128]{1,0:T(1,128)} %bitcast.28), custom_call_target="tpu_custom_call" | custom-call | flops 90194313216 | bytes 786432 | tf_op jit(solution)/shard_map/pallas_call | solution.py:63
  234.3 0.0 copy-start.1
  234.3 1.1 copy-done.1
  235.4 21.2 %shard_map.138 = bf16[192,2048]{1,0:T(8,128)(2,1)S(1)} custom-call(bf16[3072,128]{1,0:T(8,128)(2,1)S(1)} %copy-done.1), custom_call_target="tpu_custom_call" | custom-call | bytes 20000000 | tf_op jit(solution)/shard_map/pallas_call | solution.py:185
  256.6 0.0 all-gather.6.cloned.1.call-done
  256.7 2.2 convolution_reduce-precision_fusion.1
  258.8 2.2 convolution_reduce-precision_fusion.2
  261.0 0.0 copy-start.6
  261.0 2.2 convolution_reduce-precision_fusion
  263.3 0.0 copy-done.6
  263.3 3.4 %fusion.11 = bf16[192,2048]{1,0:T(8,128)(2,1)} fusion(f32[192,2048]{1,0:T(8,128)S(1)} %convolution_reduce-precision_fusion, f32[192,2048]{1,0:T(8,128)S(1)} %convolution_reduce-precision_fusion.1, f32[192,2048]{1,0:T(8,128)S(1)} %convolution_reduce-precision_fusion.2, bf16[2048,2048]{1,0:T(8,128)(2,1)} %all-gather.6.cloned.1.call-done, ...), kind=kOutput, calls=%fused_computation.18 | convolution fusion | flops 406192128 | bytes 8593408 | tf_op jit(solution)/shard_map/dot_general | solution.py:243
  (7 shorter events, 0.1 us)
Async XLA Ops:
  6.5 75.7 %copy-start = (bf16[2048,512]{1,0:T(8,128)(2,1)S(1)}, bf16[2048,512]{1,0:T(8,128)(2,1)}, u32[]{:S(2)}) copy-start(bf16[2048,512]{1,0:T(8,128)(2,1)} %param.22) | copy-start | bytes 6291460
  6.5 64.3 %copy-start.11 = (f32[4]{0:T(128)S(1)}, f32[4]{0:T(128)}, u32[]{:S(2)}) copy-start(f32[4]{0:T(128)} %param.25) | copy-start | bytes 52
  6.5 65.0 %copy-start.12 = (f32[4]{0:T(128)S(1)}, f32[4]{0:T(128)}, u32[]{:S(2)}) copy-start(f32[4]{0:T(128)} %param.26) | copy-start | bytes 52
  6.5 71.1 %copy-start.7 = (bf16[128,2048]{1,0:T(8,128)(2,1)S(1)}, bf16[128,2048]{1,0:T(8,128)(2,1)}, u32[]{:S(2)}) copy-start(bf16[128,2048]{1,0:T(8,128)(2,1)} %param.15) | copy-start | bytes 1572868
  6.5 33.6 %all-gather.4.cloned.1.call-start = ((), (), s32[]{:S(2)}) async-start(), calls=%async_computation | async-start | bytes 3932160 | tf_op jit(solution)/shard_map/all_gather | solution.py:211
  7.3 70.7 %copy-start.8 = (f32[2048]{0:T(1024)S(1)}, f32[2048]{0:T(1024)}, u32[]{:S(2)}) copy-start(f32[2048]{0:T(1024)} %param.17) | copy-start | bytes 24580
  7.3 249.4 %all-gather.6.cloned.1.call-start = ((), (), s32[]{:S(2)}) async-start(), calls=%async_computation.1 | async-start | bytes 10485760 | tf_op jit(solution)/shard_map/all_gather | solution.py:213
  77.9 3.0 %copy-start.5 = (bf16[768,2048]{1,0:T(8,128)(2,1)S(1)}, bf16[768,2048]{1,0:T(8,128)(2,1)}, u32[]{:S(2)}) copy-start(bf16[768,2048]{1,0:T(8,128)(2,1)} %all-gather.4.cloned.1.call-done) | copy-start | bytes 9437188
  82.2 2.1 copy-start.9
  84.3 2.1 copy-start.10
  148.6 1.3 copy-start.2
  149.9 1.2 copy-start.3
  151.1 0.9 copy-start.4
  234.3 1.1 copy-start.1
  261.0 2.3 copy-start.6
Sparse Core Ops, SparseCore 0:
  8.9 31.2 all-gather.3
  41.7 58.5 all-gather.5

commit v3 on v2

v3 whole, which is shorter than its diff:
```python
import functools
import math
import jax
import jax.numpy as jnp
from jax import lax
from jax.experimental import pallas as pl
from jax.experimental.pallas import tpu as pltpu
from jax.sharding import PartitionSpec as P

EPS = 1e-6
LOG2E = math.log2(math.e)


def greet(peers):
    barrier = pltpu.get_barrier_semaphore()
    for peer in peers:
        pl.semaphore_signal(barrier, inc=1, device_id=peer, device_id_type=pl.DeviceIdType.MESH)
    pl.semaphore_wait(barrier, len(peers))


def remote(source, target, send, recv, peer):
    return pltpu.make_async_remote_copy(
        src_ref=source, dst_ref=target, send_sem=send, recv_sem=recv, device_id=peer, device_id_type=pl.DeviceIdType.MESH
    )


def share(source, out, n_tp, me, send, recv, local):
    n_y, y, c = n_tp // 2, me // 2, lax.rem(me, 2)
    sibling = {"tp": y * 2 + 1 - c}
    copies = []
    if source is not None:
        copies.append(pltpu.make_async_copy(source, out.at[me], local))
    else:
        source = out.at[me]
    across = []
    for e in range(1, n_y):
        across.append(remote(source, out.at[me], send.at[0, e], recv.at[0, e], {"tp": lax.rem(y + e, n_y) * 2 + c}))
    copies.append(remote(source, out.at[me], send.at[1, 0], recv.at[1, 0], sibling))
    for copy in across + copies:
        copy.start()
    later = []
    for e in range(1, n_y):
        slot = lax.rem(y + n_y - e, n_y) * 2 + c
        later.append(remote(out.at[slot], out.at[slot], send.at[1, e], recv.at[1, e], sibling))

    def forward():
        for landing, copy in zip(across, later):
            landing.wait_recv()
            copy.start()

    def finish():
        for copy in across:
            copy.wait_send()
        for copy in copies + later:
            copy.wait()

    return forward, finish


def tp_peers(n_tp, me):
    n_y, y, c = n_tp // 2, me // 2, lax.rem(me, 2)
    return [{"tp": lax.rem(y + e, n_y) * 2 + c} for e in range(1, n_y)] + [{"tp": y * 2 + 1 - c}]


def opening_kernel(n_sp, n_tp, rows_ref, part_ref, rows_out, mods_out, ls, rs, rr, ms, mr, ps, pr):
    place, me = lax.axis_index("sp"), lax.axis_index("tp")
    around = [lax.rem(place + d, n_sp) for d in range(n_sp)]
    greet([{"sp": around[d]} for d in range(1, n_sp)] + tp_peers(n_tp, me))
    mine = mods_out.at[me, place]
    copies = [remote(part_ref, mine, ps.at[d], pr.at[d], {"sp": around[d]}) for d in range(1, n_sp)]
    copies.append(pltpu.make_async_copy(part_ref, mine, ls.at[0]))
    for copy in copies:
        copy.start()
    rows_on, rows_end = share(rows_ref, rows_out, n_tp, me, rs, rr, ls.at[1])
    for copy in copies:
        copy.wait()
    mods_on, mods_end = share(None, mods_out, n_tp, me, ms, mr, None)
    rows_on()
    mods_on()
    rows_end()
    mods_end()


def opening(latent, partials, n_sp, n_tp):
    dma = pltpu.SemaphoreType.DMA
    vm = pl.BlockSpec(memory_space=pltpu.VMEM)
    pair = dma((2, n_tp // 2))
    return pl.pallas_call(
        functools.partial(opening_kernel, n_sp, n_tp),
        in_specs=[vm] * 2,
        out_specs=[vm] * 2,
        out_shape=[
            jax.ShapeDtypeStruct((n_tp,) + latent.shape, latent.dtype),
            jax.ShapeDtypeStruct((n_tp, n_sp) + partials.shape, partials.dtype),
        ],
        scratch_shapes=[dma((2,)), pair, pair, pair, pair, dma((n_sp,)), dma((n_sp,))],
        compiler_params=pltpu.CompilerParams(collective_id=2, has_side_effects=True, vmem_limit_bytes=32 * 2**20),
        cost_estimate=pl.CostEstimate(flops=0, bytes_accessed=40_000_000, transcendentals=0),
    )(latent, partials)


def attend_kernel(cfg, lam_ref, bias_ref, gain_ref, q_ref, k_ref, v_ref, w_ref, o_ref, wo, qo, ko, vo, vt_ref, m_s, l_s, a_s, zs, zr, xs, xr, ls, ws, wr):
    split, rest, n_tp, own, width, ctx = cfg
    wide = own * width
    half = width // 2
    c = half**-0.5 * LOG2E
    place, me = lax.axis_index("sp"), lax.axis_index("tp")
    z, x = place // rest, lax.rem(place, rest)
    z_peer = [lax.rem(z + d, split) for d in range(split)]
    x_peer = [{"sp": z * rest + lax.rem(x + d, rest)} for d in range(rest)]
    greet([{"sp": z_peer[d] * rest + x} for d in range(1, split)] + x_peer[1:] + tp_peers(n_tp, me))

    def cols(index):
        return pl.ds(pl.multiple_of(index * wide, wide), wide)

    pairs = ((k_ref, ko), (v_ref, vo))
    outward = []
    for a, (src, out) in enumerate(pairs):
        for e in range(1, rest):
            outward.append(remote(src.at[:, cols(z)], out.at[place], xs.at[0, e, a], xr.at[0, e, a], x_peer[e]))
    for a, (src, out) in ((2, (q_ref, qo)),) + tuple(enumerate(pairs)):
        for d in range(1, split):
            mine = out.at[place] if a < 2 else out.at[z]
            outward.append(remote(src.at[:, cols(z_peer[d])], mine, zs.at[d, a], zr.at[d, a], {"sp": z_peer[d] * rest + x}))
    local = []
    for a, (src, out) in enumerate(pairs + ((q_ref, qo),)):
        mine = out.at[place] if a < 2 else out.at[z]
        local.append(pltpu.make_async_copy(src.at[:, cols(z)], mine, ls.at[a]))
    for copy in outward + local:
        copy.start()
    w_on, w_end = share(w_ref, wo, n_tp, me, ws, wr, ls.at[3])
    m_s[...] = jnp.full_like(m_s, -1e30)
    l_s[...] = jnp.zeros_like(l_s)
    a_s[...] = jnp.zeros_like(a_s)
    for copy in local:
        copy.wait()

    def onward(slot, d, e, a, out):
        return remote(out.at[slot], out.at[slot], xs.at[d, e, a], xr.at[d, e, a], x_peer[e] if isinstance(e, int) else x_peer[-1])

    def landed(d, a, out, slot):
        return remote(out.at[slot], out.at[slot], zs.at[d, a], zr.at[d, a], x_peer[-1])

    def absorb(j, _):
        d, e = j // rest, lax.rem(j, rest)
        from_z = lax.rem(z + split - d, split)
        slot = from_z * rest + lax.rem(x + rest - e, rest)

        @pl.when((e == 0) & (d > 0))
        def _():
            for a, (_, out) in enumerate(pairs):
                landed(d, a, out, slot).wait_recv()
                for f in range(1, rest):
                    onward(slot, d, f, a, out).start()

        @pl.when(e > 0)
        def _():
            for a, (_, out) in enumerate(pairs):
                onward(slot, d, e, a, out).wait_recv()

        @pl.when(j == split * rest // 2)
        def _():
            w_on()

        for h in range(own):
            vt_ref[...] = vo[slot, :, h * width : (h + 1) * width].T
            bias = bias_ref[h] * LOG2E

            def queries(i, _):
                zq = lax.rem(z + split - i, split)
                if h == 0:

                    @pl.when((j == 0) & (i > 0))
                    def _():
                        remote(qo.at[zq], qo.at[zq], zs.at[i, 2], zr.at[i, 2], x_peer[-1]).wait_recv()

                q = qo[zq, :, h * width : (h + 1) * width]
                k = ko[slot, :, h * width : (h + 1) * width]
                vt = vt_ref[...]
                lane = lax.broadcasted_iota(jnp.int32, q.shape, 1)
                zero = jnp.zeros_like(q)
                for m, chosen in enumerate((jnp.where(lane < half, q, zero), jnp.where(lane < half, zero, q))):
                    n = h * 2 + m
                    s = lax.dot_general(k, chosen, (((1,), (1,)), ((), ())), preferred_element_type=jnp.float32) * c
                    s = jnp.concatenate([s[:ctx] + bias, s[ctx:]], axis=0)
                    old = m_s[n, zq]
                    new = jnp.maximum(old, jnp.max(s, axis=0, keepdims=True))
                    fade = jnp.exp2(old - new)
                    p = jnp.exp2(s - new)
                    l_s[n, zq] = l_s[n, zq] * fade + jnp.sum(p, axis=0, keepdims=True)
                    a_s[n, zq] = a_s[n, zq] * fade + jnp.dot(vt, p.astype(jnp.bfloat16), preferred_element_type=jnp.float32)
                    m_s[n, zq] = new
                return 0

            lax.fori_loop(0, split, queries, 0)
        return 0

    lax.fori_loop(0, split * rest, absorb, 0)

    def close(zq, _):
        for h in range(own):
            mixed = a_s[2 * h, zq] / l_s[2 * h, zq] - lam_ref[h] * (a_s[2 * h + 1, zq] / l_s[2 * h + 1, zq])
            normed = mixed * lax.rsqrt(jnp.mean(mixed * mixed, axis=0, keepdims=True) + EPS)
            o_ref[zq, :, h * width : (h + 1) * width] = (normed.T * gain_ref[...]).astype(jnp.bfloat16)
        return 0

    lax.fori_loop(0, split, close, 0)
    for copy in outward:
        copy.wait_send()
    for d in range(1, split):
        slot = lax.rem(z + split - d, split) * rest + x
        for e in range(1, rest):
            for a, (_, out) in enumerate(pairs):
                onward(slot, d, e, a, out).wait_send()
    w_end()


def attend(q, k, v, w_out, lam, bias, gain, split, rest, n_tp, own, ctx):
    tokens, count = q.shape[0], k.shape[0]
    width = gain.shape[1]
    wide = own * width
    dma = pltpu.SemaphoreType.DMA
    vm = pl.BlockSpec(memory_space=pltpu.VMEM)
    sm = pl.BlockSpec(memory_space=pltpu.SMEM)
    stat = pltpu.VMEM((2 * own, split, 1, tokens), jnp.float32)
    return pl.pallas_call(
        functools.partial(attend_kernel, (split, rest, n_tp, own, width, ctx)),
        in_specs=[sm, sm] + [vm] * 5,
        out_specs=[vm, pl.BlockSpec(memory_space=pl.ANY)],
        out_shape=[
            jax.ShapeDtypeStruct((split, tokens, wide), q.dtype),
            jax.ShapeDtypeStruct((n_tp,) + w_out.shape, w_out.dtype),
        ],
        scratch_shapes=[
            pltpu.VMEM((split, tokens, wide), q.dtype),
            pltpu.VMEM((split * rest, count, wide), q.dtype),
            pltpu.VMEM((split * rest, count, wide), q.dtype),
            pltpu.VMEM((width, count), q.dtype),
            stat,
            stat,
            pltpu.VMEM((2 * own, split, width, tokens), jnp.float32),
            dma((split, 3)),
            dma((split, 3)),
            dma((split, rest, 2)),
            dma((split, rest, 2)),
            dma((4,)),
            dma((2, n_tp // 2)),
            dma((2, n_tp // 2)),
        ],
        compiler_params=pltpu.CompilerParams(collective_id=0, has_side_effects=True, vmem_limit_bytes=56 * 2**20),
        cost_estimate=pl.CostEstimate(flops=50_000_000_000, bytes_accessed=80_000_000, transcendentals=0),
    )(lam, bias, gain, q, k, v, w_out)


def spread_kernel(split, rest, n_tp, wide, own_rows, o_ref, out_ref, ss, rs, ls):
    place, t = lax.axis_index("sp"), lax.axis_index("tp")
    z, x = place // rest, lax.rem(place, rest)
    offsets = [(d, e) for d in range(split) for e in range(n_tp)]
    peers = {(d, e): (lax.rem(z + d, split), lax.rem(t + e, n_tp)) for d, e in offsets}
    greet([{"sp": peers[o][0] * rest + x, "tp": peers[o][1]} for o in offsets[1:]])
    mine = out_ref.at[:, pl.ds(pl.multiple_of((t * split + z) * wide, wide), wide)]
    copies = []
    for d, e in offsets:
        zp, tp = peers[d, e]
        source = o_ref.at[pl.ds(pl.multiple_of((zp * n_tp + tp) * own_rows, own_rows), own_rows), :]
        if d == 0 and e == 0:
            copies.append(pltpu.make_async_copy(source, mine, ls.at[0]))
        else:
            copies.append(remote(source, mine, ss.at[d, e], rs.at[d, e], {"sp": zp * rest + x, "tp": tp}))
        copies[-1].start()
    for copy in copies:
        copy.wait()


def spread(o, split, rest, n_tp, wide, own_rows):
    dma = pltpu.SemaphoreType.DMA
    vm = pl.BlockSpec(memory_space=pltpu.VMEM)
    return pl.pallas_call(
        functools.partial(spread_kernel, split, rest, n_tp, wide, own_rows),
        in_specs=[vm],
        out_specs=vm,
        out_shape=jax.ShapeDtypeStruct((own_rows, n_tp * split * wide), o.dtype),
        scratch_shapes=[dma((split, n_tp)), dma((split, n_tp)), dma((1,))],
        compiler_params=pltpu.CompilerParams(collective_id=1, has_side_effects=True, vmem_limit_bytes=16 * 2**20),
        cost_estimate=pl.CostEstimate(flops=0, bytes_accessed=20_000_000, transcendentals=0),
    )(o)


def modulated(inputs, norm_scale, offset_vec, scale_vec):
    rows_float = inputs.astype(jnp.float32)
    normal = rows_float * lax.rsqrt(jnp.mean(rows_float * rows_float, axis=-1, keepdims=True) + EPS)
    return (normal * norm_scale * (1.0 + scale_vec) + offset_vec).astype(jnp.bfloat16)


def per_device(sizes, latent, context, conditioning, norm_gain, mod_shift, mod_scale, mod_gate, w_query, w_key, w_value, w_out, lambdas, context_bias, head_gain):
    n_sp, n_tp = sizes
    width = head_gain.shape[0]
    heads = lambdas.shape[0]
    split = math.gcd(heads, n_sp)
    rest = n_sp // split
    own = heads // split
    place = lax.axis_index("sp")

    rows_sp = mod_shift.shape[0]
    cond_rows = lax.dynamic_slice_in_dim(conditioning, place * rows_sp, rows_sp, 1)
    activated = jax.nn.silu(cond_rows).astype(jnp.bfloat16)
    products = [jnp.dot(activated, matrix, preferred_element_type=jnp.float32) for matrix in (mod_shift, mod_scale, mod_gate)]
    partials = jnp.concatenate(products + [jnp.zeros_like(products[0])], axis=0)
    every_row, parts = opening(latent, partials, n_sp, n_tp)
    every_row = every_row.reshape(n_tp * latent.shape[0], latent.shape[1])
    summed = parts.sum(axis=1)
    modulation = jnp.moveaxis(summed, 0, 1).reshape(4, 2, -1).swapaxes(0, 1)

    context_rows = modulated(context, norm_gain, modulation[1, 0], modulation[1, 1])
    rows = modulated(every_row, norm_gain, modulation[0, 0], modulation[0, 1])
    dot = functools.partial(jnp.dot, preferred_element_type=jnp.float32)
    tokens, ctx = rows.shape[0], context_rows.shape[0]
    both = jnp.concatenate([context_rows, rows], axis=0)
    q, k, v = [
        dot(matrix, columns).astype(jnp.bfloat16) for matrix, columns in ((rows, w_query), (both, w_key), (both, w_value))
    ]
    start = (place // rest) * own
    lams = lax.dynamic_slice_in_dim(lambdas, start, own)
    biases = lax.dynamic_slice_in_dim(context_bias, start, own)
    normed, w_every = attend(q, k, v, w_out, lams, biases, head_gain.reshape(1, width), split, rest, n_tp, own, ctx)
    normed = normed.reshape(split * tokens, own * width)
    flattened = spread(normed, split, rest, n_tp, own * width, latent.shape[0])
    group = heads * width
    summed = 0.0
    for g in range(n_tp):
        partial = dot(flattened[:, g * group : (g + 1) * group], w_every[g])
        summed = summed + lax.reduce_precision(partial, 8, 7)
    attended = lax.reduce_precision(summed, 8, 7)
    return (latent.astype(jnp.float32) + modulation[0, 2] * attended).astype(jnp.bfloat16)


def solution(mesh):
    sizes = (mesh.shape["sp"], mesh.shape["tp"])
    return jax.shard_map(
        functools.partial(per_device, sizes),
        mesh=mesh,
        in_specs=(P(("sp", "tp"), None), P("sp", None), P(), P(), P("sp", "tp"), P("sp", "tp"), P("sp", "tp"),
                  P(None, "tp"), P(None, "tp"), P(None, "tp"), P("tp", None), P("tp"), P("tp"), P()),
        out_specs=P(("sp", "tp"), None),
        check_vma=False,
    )
```

time: 277 us -> 211 us (0.76)
  blocking collectives: 36.1 us -> 0 us
  waiting for transfers between devices: 30.2 us -> 0 us
  between operations: 13.7 us -> 0.16 us
  Pallas kernels: 164 us -> 175 us
  other arithmetic: 4.5 us -> 7.53 us
    all_gather x2 -> x0, blocking collectives: 36.1 us -> none  [the longest x1 30.6 us: per_device(): parts = lax.all_gather(partials, 'sp', axis=0, tiled=False).sum(axis=0)]
    all_gather x2 -> x0, waiting for transfers between devices: 29.5 us -> none  [the longest x1 29.5 us: per_device(): every_row = lax.all_gather(latent, 'tp', axis=0, tiled=True)]
    pallas_call x1, Pallas kernels: 21.2 us -> 33.4 us  [spread(): pl.pallas_call(functools.partial(spread_kernel, split, rest, n_tp, wide,...]
    dot_general x4, matrix products: 9.98 us -> 6.8 us  [per_device(): partial = dot(flattened[:, g * group:(g + 1) * group], w_every[g])]
    dot_general x3, matrix products: 5.92 us -> 8.72 us  [per_device(): dot(matrix, columns).astype(jnp.bfloat16)]
  transfers between devices with their start and end apart: 2 -> 0, of which waited for: 1 -> 0; matrix products, arithmetic and copies ran while one was open for 5% -> 0% of each run, Pallas kernels for 60% -> 0%
where the time goes in v3:
time: 211 us; the launch traced here: 208 us
  Pallas kernels  175 us (83%)
  matrix products  18.9 us (9%)
  other arithmetic  7.53 us (4%)
  local copies, waits for them, and re-layouts  6.85 us (3%)
    pallas_call x1, Pallas kernels, attend(): pl.pallas_call(functools.partial(attend_kernel, (split, rest, n_tp, own,...  113 us
    pallas_call x1, Pallas kernels, spread(): pl.pallas_call(functools.partial(spread_kernel, split, rest, n_tp, wide,...  33.4 us
    pallas_call x1, Pallas kernels, opening(): pl.pallas_call(functools.partial(opening_kernel, n_sp, n_tp), in_specs=[v...  28.9 us
    dot_general x3, matrix products, per_device(): dot(matrix, columns).astype(jnp.bfloat16)  8.72 us
    dot_general x4, matrix products, per_device(): partial = dot(flattened[:, g * group:(g + 1) * group], w_every[g])  6.8 us

profile of v3, /device:TPU:0, one launch (start us, length us, event | category | flops | bytes accessed | tf_op | source)
XLA Modules:
  0.0 208.5 jit_solution(3216262699439199193)
XLA Ops:
  0.0 0.0 copy-start
  0.0 1.4 dynamic_slice.11.bias_ref
  1.4 1.3 dynamic_slice.10.lam_ref
  2.7 0.0 copy-start.7
  2.7 1.2 fusion.23
  3.9 0.1 pad.5.clone
  4.0 1.1 fusion.39
  5.1 1.1 fusion.37
  6.2 1.1 fusion.35
  7.3 0.1 maximum_maximum_fusion.part_ref
  7.4 0.0 copy-start.2
  7.4 1.1 copy-done.2
  8.5 28.9 %shard_map.136 = (bf16[4,192,2048]{2,1,0:T(8,128)(2,1)S(1)}, f32[4,8,8,512]{3,2,1,0:T(8,128)S(1)}) custom-call(bf16[192,2048]{1,0:T(8,128)(2,1)S(1)} %copy-done.2, f32[8,512]{1,0:T(8,128)S(1)} %maximum_maximum_fusion.part_ref), custom_call_target="tpu_custom_call" | custom-call | bytes 40000000 | tf_op jit(solution)/shard_map/pallas_call | solution.py:88
  37.4 0.0 copy-start.1
  37.4 1.6 copy-done.1
  39.2 0.1 reshape.55
  39.3 2.6 %multiply_reduce_fusion = f32[4,192]{1,0:T(4,128)S(1)} fusion(bf16[4,192,2048]{2,1,0:T(8,128)(2,1)} %copy-done.1), kind=kLoop, calls=%fused_computation.5 | loop fusion | flops 4717824 | bytes 3148800 | tf_op jit(solution)/shard_map/reduce_sum | solution.py:291
  41.9 0.1 rsqrt.20
  42.0 0.0 copy-done.7
  42.0 0.0 copy-start.6
  42.0 0.0 copy-start.8
  42.0 3.3 %fusion.3 = bf16[768,2048]{1,0:T(8,128)(2,1)S(1)} fusion(f32[2048]{0:T(1024)S(1)} %bitcast.44, f32[2048]{0:T(1024)S(1)} %bitcast.45, f32[2048]{0:T(1024)S(1)} %copy-done.7, f32[768]{0:T(1024)S(1)} %rsqrt.20, bf16[4,192,2048]{2,1,0:T(8,128)(2,1)} %copy-done.1), kind=kLoop, calls=%fused_computation.4 | loop fusion | flops 9437184 | bytes 6319104 | tf_op jit(solution)/shard_map/convert_element_type | solution.py:292
  45.2 0.0 copy-done.6
  45.3 0.3 fusion.27
  45.5 0.0 copy-done.8
  45.5 2.7 %convolution_convert_fusion.q_ref = bf16[768,512]{1,0:T(8,128)(2,1)} fusion(bf16[768,2048]{1,0:T(8,128)(2,1)S(1)} %fusion.3, bf16[2048,512]{1,0:T(8,128)(2,1)S(1)} %copy-done.8), kind=kOutput, calls=%fused_computation.30 | convolution fusion | flops 1611005952 | bytes 6029312 | tf_op jit(solution)/shard_map/dot_general | solution.py:320
  48.2 0.0 copy-done
  48.2 0.0 copy-start.9
  48.2 3.0 %fusion.22.v_ref = bf16[896,512]{1,0:T(8,128)(2,1)} fusion(bf16[2048,512]{1,0:T(8,128)(2,1)S(1)} %copy-done, bf16[768,2048]{1,0:T(8,128)(2,1)S(1)} %fusion.3, bf16[128,2048]{1,0:T(8,128)(2,1)S(1)} %fusion.27), kind=kOutput, calls=%fused_computation.29 | convolution fusion | flops 1886846976 | bytes 6684672 | tf_op jit(solution)/shard_map/dot_general | solution.py:320
  51.2 0.0 copy-done.9
  51.2 3.0 %fusion.21.k_ref = bf16[896,512]{1,0:T(8,128)(2,1)} fusion(bf16[2048,512]{1,0:T(8,128)(2,1)S(1)} %copy-done.9, bf16[768,2048]{1,0:T(8,128)(2,1)S(1)} %fusion.3, bf16[128,2048]{1,0:T(8,128)(2,1)S(1)} %fusion.27), kind=kOutput, calls=%fused_computation.28 | convolution fusion | flops 1886846976 | bytes 6684672 | tf_op jit(solution)/shard_map/dot_general | solution.py:320
  54.3 112.8 %shard_map.137 = (bf16[4,768,128]{2,1,0:T(8,128)(2,1)}, bf16[4,512,2048]{2,1,0:T(8,128)(2,1)}) custom-call(f32[1]{0:T(128)} %dynamic_slice.10.lam_ref, f32[1]{0:T(128)} %dynamic_slice.11.bias_ref, f32[1,128]{1,0:T(1,128)} %bitcast.46, bf16[768,512]{1,0:T(8,128)(2,1)} %convolution_convert_fusion.q_ref, bf16[896,512]{1,0:T(8,128)(2,1)} %fusion.21.k_ref, ...), custom_call_target="tpu_custom_call" | custom-call | flops 49999998976 | bytes 80000000 | tf_op jit(solution)/shard_map/pallas_call | solution.py:226
  167.1 0.0 copy-start.4
  167.1 1.1 copy-done.4
  168.2 0.0 copy-start.5
  168.2 33.4 %shard_map.138 = bf16[192,2048]{1,0:T(8,128)(2,1)S(1)} custom-call(bf16[3072,128]{1,0:T(8,128)(2,1)S(1)} %bitcast.38), custom_call_target="tpu_custom_call" | custom-call | bytes 20000000 | tf_op jit(solution)/shard_map/pallas_call | solution.py:278
  201.6 2.2 %convolution_reduce-precision_fusion = f32[192,2048]{1,0:T(8,128)S(1)} fusion(bf16[4,512,2048]{2,1,0:T(8,128)(2,1)} %get-tuple-element.12, bf16[192,2048]{1,0:T(8,128)(2,1)S(1)} %shard_map.138), kind=kOutput, calls=%fused_computation.7 | convolution fusion | flops 403046400 | bytes 3866624 | tf_op jit(solution)/shard_map/dot_general | solution.py:331
  203.8 0.0 copy-start.3
  203.8 2.3 %convolution_reduce-precision_fusion.1 = f32[192,2048]{1,0:T(8,128)S(1)} fusion(bf16[4,512,2048]{2,1,0:T(8,128)(2,1)} %get-tuple-element.12, bf16[192,2048]{1,0:T(8,128)(2,1)S(1)} %shard_map.138), kind=kOutput, calls=%fused_computation.8 | convolution fusion | flops 403046400 | bytes 3866624 | tf_op jit(solution)/shard_map/dot_general | solution.py:331
  206.1 0.0 copy-done.5
  206.1 0.6 convolution_reduce-precision_fusion.2
  206.7 0.0 copy-done.3
  206.7 1.8 fusion.10
  (6 shorter events, 0.1 us)
Async XLA Ops:
  0.0 48.2 %copy-start = (bf16[2048,512]{1,0:T(8,128)(2,1)S(1)}, bf16[2048,512]{1,0:T(8,128)(2,1)}, u32[]{:S(2)}) copy-start(bf16[2048,512]{1,0:T(8,128)(2,1)} %param.23) | copy-start | bytes 6291460
  2.7 39.3 %copy-start.7 = (f32[2048]{0:T(1024)S(1)}, f32[2048]{0:T(1024)}, u32[]{:S(2)}) copy-start(f32[2048]{0:T(1024)} %param.17) | copy-start | bytes 24580
  7.4 1.1 copy-start.2
  37.4 1.6 copy-start.1
  42.0 3.3 %copy-start.6 = (bf16[128,2048]{1,0:T(8,128)(2,1)S(1)}, bf16[128,2048]{1,0:T(8,128)(2,1)}, u32[]{:S(2)}) copy-start(bf16[128,2048]{1,0:T(8,128)(2,1)} %param.15) | copy-start | bytes 1572868
  42.0 3.6 %copy-start.8 = (bf16[2048,512]{1,0:T(8,128)(2,1)S(1)}, bf16[2048,512]{1,0:T(8,128)(2,1)}, u32[]{:S(2)}) copy-start(bf16[2048,512]{1,0:T(8,128)(2,1)} %param.21) | copy-start | bytes 6291460
  48.2 3.0 %copy-start.9 = (bf16[2048,512]{1,0:T(8,128)(2,1)S(1)}, bf16[2048,512]{1,0:T(8,128)(2,1)}, u32[]{:S(2)}) copy-start(bf16[2048,512]{1,0:T(8,128)(2,1)} %param.22) | copy-start | bytes 6291460
  167.1 1.1 copy-start.4
  168.2 37.9 %copy-start.5 = (bf16[4,512,2048]{2,1,0:T(8,128)(2,1)S(1)}, bf16[4,512,2048]{2,1,0:T(8,128)(2,1)}, u32[]{:S(2)}) copy-start(bf16[4,512,2048]{2,1,0:T(8,128)(2,1)} %get-tuple-element.12) | copy-start | bytes 25165828
  203.8 2.9 %copy-start.3 = (bf16[192,2048]{1,0:T(8,128)(2,1)S(1)}, bf16[192,2048]{1,0:T(8,128)(2,1)}, u32[]{:S(2)}) copy-start(bf16[192,2048]{1,0:T(8,128)(2,1)} %rows_ref.1) | copy-start | bytes 2359300
